TPU v7x, 32 devices: a whole 2x2x4 slice. The times are simulated.
32 devices in a mesh: sp: 8 (over z, x), tp: 4 (over y, core).
Axes of the slice: x: 2, y: 2, z: 4, core: 2. Of those that a mesh axis runs over, the one named last changes fastest.
Arguments:
- tokens: bfloat16 [3072, 2048], P('sp', 'tp'), may hold values from -6 to 6
- pre_gain: float32 [2048], replicated, may hold values from 0.1 to 1.9
- outer_gate_weight: bfloat16 [2048, 1024], P(None, 'tp'), may hold values from -0.125 to 0.125
- inner_gate_weight: bfloat16 [2048, 1024], P(None, 'tp'), may hold values from -0.125 to 0.125
- source_weight: bfloat16 [2048, 1024], P(None, 'tp'), may hold values from -0.125 to 0.125
- conv_taps: bfloat16 [3, 1024], P(None, 'tp'), may hold values from -3.5 to 3.5
- q_down_weight: bfloat16 [2048, 768], replicated, may hold values from -0.125 to 0.125
- q_norm_gain: float32 [768], replicated, may hold values from 0.5 to 16
- q_up_weight: bfloat16 [768, 3072], P(None, 'tp'), may hold values from -0.21875 to 0.21875
- kv_down_weight: bfloat16 [2048, 512], replicated, may hold values from -0.125 to 0.125
- rope_key_weight: bfloat16 [2048, 32], replicated, may hold values from -0.125 to 0.125
- kv_norm_gain: float32 [512], replicated, may hold values from 0.5 to 16
- kv_up_weight: bfloat16 [512, 4096], P(None, 'tp'), may hold values from -0.25 to 0.25
- attn_out_weight: bfloat16 [2048, 2048], P('tp'), may hold values from -4 to 4
- conv_out_weight: bfloat16 [1024, 2048], P('tp'), may hold values from -0.1875 to 0.1875
- post_gain: float32 [2048], P('tp'), may hold values from 0.1 to 1.9
Outputs:
- mixed: bfloat16 [3072, 2048], P('sp', 'tp')
- log_total: float32 [32, 3072], P('tp', 'sp')
All inputs are finite; a program needn't handle non-finite values.
Results may differ from a plain program's by a relative error of at most 0.017.
The roundings to bfloat16 on the way count: a program that leaves them out, or rounds other values in their place, can miss the bound.
Values may be sent and summed in bfloat16 or wider, within the bound.
A program may use at most 128 MiB of HBM per device.

v0:
```python
import functools
import math

import jax
import jax.numpy as jnp
from jax import lax
from jax.experimental import pallas as pl
from jax.experimental.pallas import tpu as pltpu
from jax.sharding import PartitionSpec as P

NOPE = 64
ROPE = 32
VDIM = 64
TAPS = 3
LANES = 128

EPSILON = 1e-06
THETA = 500000.0
NEGATIVE = -1e30
MESH = pl.DeviceIdType.MESH
BF = jnp.bfloat16
F32 = jnp.float32


def remote(src, dst, send, recv, **where):
    return pltpu.make_async_remote_copy(
        src_ref=src, dst_ref=dst, send_sem=send, recv_sem=recv, device_id=where, device_id_type=MESH
    )


def dot(a, b):
    return jnp.dot(a, b, preferred_element_type=F32)


def greet_tp(tp, n):
    barrier = pltpu.get_barrier_semaphore()
    for step in range(1, n):
        pl.semaphore_signal(
            barrier, inc=1, device_id={"tp": lax.rem(tp + step, n)}, device_id_type=MESH
        )
    pl.semaphore_wait(barrier, n - 1)


def project_kernel(
    n, chunk,
    tok, pre, qg, kg, cos, sin, wo, wi, ws, wq, wk, wr,
    outer, driven, qn, kvb,
    buf, vo, vi, vs, vq, vk, vr, wsem, own_s, own_r, y_s, y_r, f_s, f_r,
):
    tp = lax.axis_index("tp")
    ny = n // 2
    y, core = tp // 2, lax.rem(tp, 2)
    partner = tp + 1 - 2 * core
    rows, width = tok.shape
    count = rows // chunk
    loads = [
        pltpu.make_async_copy(a, b, wsem.at[i])
        for i, (a, b) in enumerate(((wo, vo), (wi, vi), (ws, vs), (wq, vq), (wk, vk), (wr, vr)))
    ]
    greet_tp(tp, n)

    def part(r):
        return pl.ds(r * chunk, chunk)

    def y_copy(r, step):
        to = lax.rem(y + step, ny) * 2 + core
        return remote(
            tok.at[part(r)], buf.at[tp, part(r)], y_s.at[r, step], y_r.at[r, y], tp=to
        )

    def y_arrival(r, other):
        return remote(
            tok.at[part(r)], buf.at[other * 2 + core, part(r)], y_s.at[r, 0], y_r.at[r, other],
            tp=partner,
        )

    def own_copy(r):
        return remote(tok.at[part(r)], buf.at[tp, part(r)], own_s.at[r], own_r.at[r], tp=partner)

    def forward(r, other):
        here = buf.at[other * 2 + core, part(r)]
        return remote(here, here, f_s.at[r, other], f_r.at[r, other], tp=partner)

    for r in range(count):
        for step in range(1, ny):
            y_copy(r, step).start()
    for r in range(count):
        own_copy(r).start()
    for load in loads:
        load.start()
    buf[tp] = tok[...]
    for load in loads:
        load.wait()

    def compute(r, carry):
        for step in range(1, ny):
            other = lax.rem(y + ny - step, ny)
            y_arrival(r, other).wait_recv()
            forward(r, other).start()
        own_copy(r).wait_recv()
        for step in range(1, ny):
            other = lax.rem(y + ny - step, ny)
            forward(r, other).wait_recv()
        here = pl.ds(pl.multiple_of(r * chunk, chunk), chunk)
        total = n * width
        wide = jnp.concatenate([buf[s, here] for s in range(n)], axis=1).astype(F32)
        factor = lax.rsqrt(jnp.sum(wide * wide, axis=1, keepdims=True) / total + EPSILON)
        scaled = (wide * pre[...]).astype(BF)
        kv = dot(scaled, vk[...]) * factor
        kv = kv * lax.rsqrt(jnp.mean(kv * kv, axis=1, keepdims=True) + EPSILON) * kg[...]
        rank = kv.shape[1]
        kvb[here, :rank] = kv.astype(BF)
        turn = factor * lax.dot_general(
            scaled, vr[...], (((1,), (1,)), ((), ())), preferred_element_type=F32
        )
        swapped = jnp.concatenate([turn[:, ROPE // 2 :], turn[:, : ROPE // 2]], axis=1)
        turn = turn * cos[:, here].T + swapped * sin[:, here].T
        kvb[here, rank:] = jnp.concatenate(
            [turn, jnp.zeros((chunk, LANES - ROPE), F32)], axis=1
        ).astype(BF)
        q = dot(scaled, vq[...]) * factor
        q = q * lax.rsqrt(jnp.mean(q * q, axis=1, keepdims=True) + EPSILON) * qg[...]
        qn[here] = q.astype(BF)
        outer[here] = (dot(scaled, vo[...]) * factor).astype(BF)
        inner = (dot(scaled, vi[...]) * factor).astype(BF).astype(F32)
        source = (dot(scaled, vs[...]) * factor).astype(BF).astype(F32)
        driven[here] = (inner * source).astype(BF)
        return carry

    lax.fori_loop(0, count, compute, 0)
    for r in range(count):
        own_copy(r).wait_send()
        for step in range(1, ny):
            y_copy(r, step).wait_send()
            forward(r, lax.rem(y + step, ny)).wait_send()


def attend_kernel(
    nz, nx, ntp, heads,
    kvb, qt, up,
    att, logs,
    buf, kv, acc, top, low, z_s, x_s, d_s, i_r, d_r,
):
    sp, tp = lax.axis_index("sp"), lax.axis_index("tp")
    z, x = sp // nx, lax.rem(sp, nx)
    core = lax.rem(tp, 2)
    partner = tp + 1 - 2 * core
    rows = kvb.shape[0]
    half = rows // 2
    rank = up.shape[0]
    scale = (NOPE + ROPE) ** (-0.5)
    factor = scale * math.log2(math.e)
    mine = pl.ds(pl.multiple_of(core * half, half), half)

    barrier = pltpu.get_barrier_semaphore()

    def greet(**where):
        pl.semaphore_signal(barrier, inc=1, device_id=where, device_id_type=MESH)

    greet(tp=partner)
    for step in range(1, nx):
        greet(sp=z * nx + lax.rem(x + step, nx))

    @pl.when(z > 0)
    def _():
        greet(sp=sp - nx)

    @pl.when(z < nz - 1)
    def _():
        greet(sp=sp + nx)

    inside = jnp.where(z > 0, 1, 0) + jnp.where(z < nz - 1, 1, 0)
    pl.semaphore_wait(barrier, nx + inside)

    def up_copy(k):
        src = sp - k * nx
        return remote(buf.at[src, mine], buf.at[src, mine], z_s.at[k], i_r.at[src], sp=sp + nx)

    def side_copy(k, step):
        src = sp - k * nx
        to = z * nx + lax.rem(x + step, nx)
        return remote(buf.at[src, mine], buf.at[src, mine], x_s.at[k, step], i_r.at[src], sp=to)

    def own_up():
        return remote(kvb.at[mine], buf.at[sp, mine], z_s.at[0], i_r.at[sp], sp=sp + nx)

    def own_side(step):
        to = z * nx + lax.rem(x + step, nx)
        return remote(kvb.at[mine], buf.at[sp, mine], x_s.at[0, step], i_r.at[sp], sp=to)

    def arrival(src):
        return remote(kvb.at[mine], buf.at[src, mine], z_s.at[0], i_r.at[src], tp=partner)

    def share(src):
        return remote(buf.at[src, mine], buf.at[src, mine], d_s.at[src], d_r.at[src], tp=partner)

    @pl.when(z < nz - 1)
    def _():
        own_up().start()

    for step in range(1, nx):
        @pl.when(x + step < nx)
        def _(step=step):
            own_side(step).start()

    def compute(block, first):
        lat = block[:, :rank]
        turn = block[:, rank:]
        for h in range(0, heads, 2):
            both = dot(lat, up[:, h * LANES : (h + 2) * LANES]).astype(BF)
            kv[h] = both[:, :LANES]
            kv[h + 1] = both[:, LANES:]

        def one(h):
            keyval = kv[h]
            scores = dot(jnp.concatenate([keyval, turn], axis=1), qt[h])
            if first:
                key = lax.broadcasted_iota(jnp.int32, scores.shape, 0)
                query = lax.broadcasted_iota(jnp.int32, scores.shape, 1)
                scores = jnp.where(key <= query, scores, NEGATIVE)
            peak = jnp.max(scores, axis=0, keepdims=True) * factor
            if not first:
                before = top[h]
                peak = jnp.maximum(before, peak)
            weights = jnp.exp2(scores * factor - peak)
            total = jnp.sum(weights, axis=0, keepdims=True)
            values = lax.dot_general(
                keyval, weights.astype(BF), (((0,), (0,)), ((), ())), preferred_element_type=F32
            )
            if not first:
                shrink = jnp.exp2(before - peak)
                total = total + low[h] * shrink
                values = values + acc[h] * shrink
            top[h] = peak
            low[h] = total
            acc[h] = values

        def pair(i, carry):
            one(2 * i)
            one(2 * i + 1)
            return carry

        lax.fori_loop(0, heads // 2, pair, 0)

    compute(kvb[...], True)

    def side_source(k, step):
        return (z - k) * nx + lax.rem(x + step, nx)

    def side_share(k, low_step):
        def run(step, carry):
            src = side_source(k, step)
            arrival(src).wait_recv()
            share(src).start()
            return carry

        lax.fori_loop(low_step, nx, run, 0)

    def shared_compute(src):
        share(src).wait_recv()
        compute(buf[src], False)

    def level(k, carry):
        src = sp - k * nx
        fresh = k <= z

        @pl.when(fresh)
        def _():
            arrival(src).wait_recv()
            share(src).start()

            @pl.when(z < nz - 1)
            def _():
                up_copy(k).start()

            for step in range(1, nx):
                side_copy(k, step).start()

        low_step = jnp.where(k == 1, nx - x, 1)
        side_share(k - 1, low_step)

        def run(step, carry):
            shared_compute(jnp.where(step == 0, src, side_source(k - 1, step + low_step - 1)))
            return carry

        lax.fori_loop(jnp.where(fresh, 0, 1), nx - low_step + 1, run, 0)
        return carry

    lax.fori_loop(1, z + 2, level, 0)

    for i in range(heads // 2):
        both = jnp.concatenate(
            [acc[2 * i, NOPE:] / low[2 * i], acc[2 * i + 1, NOPE:] / low[2 * i + 1]], axis=0
        )
        att[:, i * LANES : (i + 1) * LANES] = both.T.astype(BF)
    for h in range(heads):
        logs[h : h + 1, :] = top[h] * math.log(2.0) + jnp.log(low[h])

    @pl.when(z < nz - 1)
    def _():
        own_up().wait_send()

    for step in range(1, nx):
        @pl.when(x + step < nx)
        def _(step=step):
            own_side(step).wait_send()

    def side_sent(k, low_step):
        def run(step, carry):
            share((z - k) * nx + lax.rem(x + step, nx)).wait_send()
            return carry

        lax.fori_loop(low_step, nx, run, 0)

    side_sent(0, nx - x)

    def sent(k, carry):
        @pl.when(z < nz - 1)
        def _():
            up_copy(k).wait_send()

        for step in range(1, nx):
            side_copy(k, step).wait_send()
        share(sp - k * nx).wait_send()
        side_sent(k, 1)
        return carry

    lax.fori_loop(1, z + 1, sent, 0)


def finish_kernel(
    n, chunk,
    att, conv, wa, wc, gain,
    out,
    away, mine, pin, ysend, yin, peer, pown, total, sq, sqin,
    a_s, a_r, y_s, y_r, p_s, p_r, q_s, q_r,
):
    tp = lax.axis_index("tp")
    ny = n // 2
    y, core = tp // 2, lax.rem(tp, 2)
    partner = tp + 1 - 2 * core
    rows, width = out.shape
    count = rows // chunk
    greet_tp(tp, n)

    def part(r):
        return pl.ds(r * chunk, chunk)

    def product(r, dest):
        columns = pl.ds(pl.multiple_of(dest * width, width), width)
        return (dot(att[part(r)], wa[:, columns]) + dot(conv[part(r)], wc[:, columns])).astype(BF)

    def to_partner(r, step):
        return remote(
            away.at[step, part(r)], pin.at[step, part(r)], a_s.at[r, step], a_r.at[r, step], tp=partner
        )

    def across(r, step):
        to = lax.rem(y + step, ny) * 2 + core
        return remote(
            ysend.at[step, part(r)], yin.at[step, part(r)], y_s.at[r, step], y_r.at[r, step], tp=to
        )

    def home(r):
        return remote(peer.at[part(r)], pown.at[part(r)], p_s.at[r], p_r.at[r], tp=partner)

    def squares(step):
        return remote(
            sq, sqin.at[step], q_s.at[step], q_r.at[step], tp=lax.rem(tp + step, n)
        )

    for r in range(count):
        for step in range(1, ny):
            dest = lax.rem(y + step, ny) * 2
            away[step, part(r)] = product(r, dest + 1 - core)
            to_partner(r, step).start()
            mine[step, part(r)] = product(r, dest + core)
    for r in range(count):
        for step in range(1, ny):
            to_partner(r, step).wait_recv()
            ysend[step, part(r)] = (
                mine[step, part(r)].astype(F32) + pin[step, part(r)].astype(F32)
            ).astype(BF)
            across(r, step).start()
    for r in range(count):
        peer[part(r)] = product(r, partner)
        home(r).start()
        total[part(r)] = product(r, tp).astype(F32)
    for r in range(count):
        home(r).wait_recv()
        total[part(r)] += pown[part(r)].astype(F32)
    for r in range(count):
        for step in range(1, ny):
            across(r, step).wait_recv()
            total[part(r)] += yin[step, part(r)].astype(F32)
        value = total[part(r)]
        sums = jnp.sum(value * value, axis=1, keepdims=True)
        sq[:, part(r)] = jnp.broadcast_to(sums, (chunk, LANES)).T[:8]
    for step in range(1, n):
        squares(step).start()
    whole = sq[...]
    for step in range(1, n):
        squares(step).wait_recv()
        whole = whole + sqin[step]
    scale = lax.rsqrt(whole / (n * width) + EPSILON)
    for r in range(count):
        column = jnp.broadcast_to(
            scale[:1, r * chunk : (r + 1) * chunk], (LANES, chunk)
        ).T[:, :1]
        out[part(r)] = (total[part(r)] * column * gain[...]).astype(BF)
    for r in range(count):
        home(r).wait_send()
        for step in range(1, ny):
            to_partner(r, step).wait_send()
            across(r, step).wait_send()
    for step in range(1, n):
        squares(step).wait_send()


def vmem(count):
    return [pl.BlockSpec(memory_space=pltpu.VMEM)] * count


def params(collective):
    return pltpu.CompilerParams(
        collective_id=collective, has_side_effects=True, vmem_limit_bytes=56 * 1024 * 1024
    )


DMA = pltpu.SemaphoreType.DMA


def body(
    nsp, ntp,
    tokens, pre_gain, outer_gate_weight, inner_gate_weight, source_weight, conv_taps,
    q_down_weight, q_norm_gain, q_up_weight, kv_down_weight, rope_key_weight, kv_norm_gain,
    kv_up_weight, attn_out_weight, conv_out_weight, post_gain,
):
    rows, width = tokens.shape
    ny = ntp // 2
    nx = ny if nsp % ny == 0 else 1
    nz = nsp // nx
    chunk = LANES
    count = rows // chunk
    q_rank, kv_rank = q_down_weight.shape[1], kv_down_weight.shape[1]
    channels = outer_gate_weight.shape[1]
    heads = q_up_weight.shape[1] // (NOPE + ROPE)
    struct = jax.ShapeDtypeStruct
    sp = lax.axis_index("sp")

    pos = (sp * rows + jnp.arange(rows, dtype=jnp.int32)).astype(F32)
    freqs = THETA ** (-jnp.arange(0, ROPE, 2, dtype=F32) / ROPE)
    angles = freqs[:, None] * pos[None, :]
    cosine, sine = jnp.cos(angles), jnp.sin(angles)
    cos_full = jnp.concatenate([cosine, cosine], axis=0)
    sin_full = jnp.concatenate([-sine, sine], axis=0)

    weights = (
        outer_gate_weight, inner_gate_weight, source_weight,
        q_down_weight, kv_down_weight, rope_key_weight.T,
    )
    outer, driven, q_normed, kvb = pl.pallas_call(
        functools.partial(project_kernel, ntp, chunk),
        out_shape=[
            struct((rows, channels), BF), struct((rows, channels), BF),
            struct((rows, q_rank), BF), struct((rows, kv_rank + LANES), BF),
        ],
        in_specs=vmem(6) + [pl.BlockSpec(memory_space=pl.ANY)] * 6,
        out_specs=vmem(4),
        scratch_shapes=[pltpu.VMEM((ntp, rows, width), BF)]
        + [pltpu.VMEM(w.shape, BF) for w in weights]
        + [
            DMA((6,)), DMA((count,)), DMA((count,)), DMA((count, ny)), DMA((count, ny)),
            DMA((count, ny)), DMA((count, ny)),
        ],
        compiler_params=params(0),
        name="project",
    )(
        tokens, pre_gain[None], q_norm_gain[None], kv_norm_gain[None], cos_full, sin_full, *weights
    )

    query = lax.dot_general(
        q_up_weight, q_normed, (((0,), (1,)), ((), ())), preferred_element_type=F32
    ).reshape(heads, NOPE + ROPE, rows)
    first, second = query[:, NOPE : NOPE + ROPE // 2], query[:, NOPE + ROPE // 2 :]
    ct, st = cosine[None], sine[None]
    qt = jnp.concatenate(
        [
            query[:, :NOPE], jnp.zeros((heads, VDIM, rows), F32),
            first * ct - second * st, second * ct + first * st,
            jnp.zeros((heads, LANES - ROPE, rows), F32),
        ],
        axis=1,
    ).astype(BF)

    attended, log_total = pl.pallas_call(
        functools.partial(attend_kernel, nz, nx, ntp, heads),
        out_shape=[struct((rows, heads * VDIM), BF), struct((heads, rows), F32)],
        in_specs=vmem(3),
        out_specs=vmem(2),
        scratch_shapes=[
            pltpu.VMEM((nsp, rows, kv_rank + LANES), BF),
            pltpu.VMEM((heads, rows, LANES), BF),
            pltpu.VMEM((heads, LANES, rows), F32),
            pltpu.VMEM((heads, 1, rows), F32),
            pltpu.VMEM((heads, 1, rows), F32),
            DMA((nz,)), DMA((nz, nx)), DMA((nsp,)), DMA((nsp,)), DMA((nsp,)),
        ],
        compiler_params=params(1),
        name="attend",
    )(kvb, qt, kv_up_weight)

    prior = lax.ppermute(driven[rows - (TAPS - 1) :], "sp", [(i, i + 1) for i in range(nsp - 1)])
    extended = jnp.concatenate([prior, driven], axis=0)
    convolved = jnp.zeros(driven.shape, F32)
    for index in range(TAPS):
        convolved = convolved + conv_taps[index].astype(F32) * extended[
            index : index + rows
        ].astype(F32)
    conv_branch = (outer.astype(F32) * convolved).astype(BF)

    block = (ny, rows, width)
    mixed = pl.pallas_call(
        functools.partial(finish_kernel, ntp, chunk),
        out_shape=struct((rows, width), BF),
        in_specs=vmem(5),
        out_specs=pl.BlockSpec(memory_space=pltpu.VMEM),
        scratch_shapes=[pltpu.VMEM(block, BF)] * 5
        + [
            pltpu.VMEM((rows, width), BF), pltpu.VMEM((rows, width), BF),
            pltpu.VMEM((rows, width), F32),
            pltpu.VMEM((8, rows), F32), pltpu.VMEM((ntp, 8, rows), F32),
            DMA((count, ny)), DMA((count, ny)), DMA((count, ny)), DMA((count, ny)),
            DMA((count,)), DMA((count,)), DMA((ntp,)), DMA((ntp,)),
        ],
        compiler_params=params(2),
        name="finish",
    )(attended, conv_branch, attn_out_weight, conv_out_weight, post_gain[None])
    return mixed, log_total


def solution(mesh):
    placed = (
        P("sp", "tp"), P(), P(None, "tp"), P(None, "tp"), P(None, "tp"), P(None, "tp"), P(), P(),
        P(None, "tp"), P(), P(), P(), P(None, "tp"), P("tp", None), P("tp", None), P("tp"),
    )
    return jax.shard_map(
        functools.partial(body, mesh.shape["sp"], mesh.shape["tp"]),
        mesh=mesh,
        in_specs=placed,
        out_specs=(P("sp", "tp"), P("tp", "sp")),
        check_vma=False,
    )
```

profile of v0, /device:TPU:27, one launch (start us, length us, event | category | flops | bytes accessed | tf_op | source)
XLA Modules:
  0.0 101.3 jit_solution(9999781166171826950)
XLA Ops:
  0.6 0.0 copy-start
  0.7 1.4 %broadcast_in_dim.26.qg = f32[1,768]{1,0:T(1,128)} reshape(f32[768]{0:T(1024)} %param.23) | data formatting | bytes 6144 | tf_op jit(solution)/shard_map/broadcast_in_dim | solution.py:479
  2.0 0.2 fusion.4
  2.2 0.0 copy-start.2
  2.2 0.0 copy-start.4
  2.2 0.6 copy-done.2
  2.8 0.6 pad_maximum_fusion.1
  3.5 0.0 copy-done.4
  3.5 0.0 copy-start.9
  3.5 16.8 %project.1 = (bf16[384,256]{1,0:T(8,128)(2,1)}, bf16[384,256]{1,0:T(8,128)(2,1)}, bf16[384,768]{1,0:T(8,128)(2,1)}, bf16[384,640]{1,0:T(8,128)(2,1)}) custom-call(bf16[384,512]{1,0:T(8,128)(2,1)} %tok.1, f32[1,2048]{1,0:T(1,128)} %bitcast.16, f32[1,768]{1,0:T(1,128)} %broadcast_in_dim.26.qg, f32[1,512]{1,0:T(1,128)} %bitcast.21, ...), custom_call_target="tpu_custom_call" | custom-call | tf_op jit(solution)/shard_map/project/pallas_call | solution.py:462
  20.3 1.2 %slice.32 = bf16[2,256]{1,0:T(2,128)(2,1)} slice(bf16[384,256]{1,0:T(8,128)(2,1)} %get-tuple-element.12), slice={[382:384], [0:256]} | slice | bytes 2048 | tf_op jit(solution)/shard_map/slice | solution.py:513
  21.5 1.3 %collective-permute-start = (bf16[2,256]{1,0:T(2,128)(2,1)}, bf16[2,256]{1,0:T(2,128)(2,1)S(1)}, u32[]{:S(2)}, u32[]{:S(2)}) collective-permute-start(bf16[2,256]{1,0:T(2,128)(2,1)} %slice.32), channel_id=1, source_target_pairs={{0,4},{4,8},{8,12},{12,16},{16,20},{20,24},{24,28},{1,5},{5,9},{9,... | collective-permute-start | bytes 3080 | tf_op jit(solution)/shard_map/ppermute | solution.py:513
  22.8 0.0 copy-done.9
  22.9 0.0 copy-done
  22.9 1.7 %convolution_bitcast_fusion = f32[768,384]{0,1:T(8,128)S(1)} fusion(bf16[384,768]{1,0:T(8,128)(2,1)} %get-tuple-element.9, bf16[768,768]{1,0:T(8,128)(2,1)S(1)} %copy-done), kind=kOutput, calls=%fused_computation | convolution fusion | flops 452984832 | bytes 2949120 | tf_op jit(solution)/shard_map/dot_general | solution.py:482
  24.6 0.4 copy.18
  24.9 0.0 copy-start.3
  24.9 0.0 copy-start.5
  25.0 0.1 broadcast_dynamic-update-slice_fusion.1
  25.1 0.8 fusion.2
  25.9 0.0 copy-done.3
  25.9 0.0 copy-done.5
  25.9 0.1 broadcast_dynamic-update-slice_fusion.qt
  26.0 0.0 copy-start.1
  26.0 0.0 copy-start.6
  26.0 0.0 copy-start.7
  26.1 1.1 %copy-done.1 = bf16[8,256,384]{2,1,0:T(8,128)(2,1)} copy-done((bf16[8,256,384]{2,1,0:T(8,128)(2,1)}, bf16[8,256,384]{2,1,0:T(8,128)(2,1)S(1)}, u32[]{:S(2)}) %copy-start.1) | copy-done | bytes 1572888
  27.2 50.4 %attend.1 = (bf16[384,512]{1,0:T(8,128)(2,1)}, f32[8,384]{1,0:T(8,128)}) custom-call(bf16[384,640]{1,0:T(8,128)(2,1)} %get-tuple-element.8.kvb, bf16[8,256,384]{2,1,0:T(8,128)(2,1)} %copy-done.1, bf16[512,1024]{1,0:T(8,128)(2,1)} %up.1), custom_call_target="tpu_custom_call" | custom-call | tf_op jit(solution)/shard_map/attend/pallas_call | solution.py:496
  77.6 0.0 collective-permute-done
  77.6 0.0 copy-done.6
  77.6 0.0 copy-done.7
  77.6 0.8 multiply_convert_fusion.conv
  78.5 0.0 copy-start.8
  78.5 20.5 %finish.1 = bf16[384,512]{1,0:T(8,128)(2,1)} custom-call(bf16[384,512]{1,0:T(8,128)(2,1)} %get-tuple-element.10.att, bf16[384,256]{1,0:T(8,128)(2,1)} %multiply_convert_fusion.conv, bf16[512,2048]{1,0:T(8,128)(2,1)} %wa.1, bf16[256,2048]{1,0:T(8,128)(2,1)} %wc.1, f32[1,512]{1,0:T(1,128)} %bitcast.20), custom_call_target="tpu_custom_call" | custom-call | tf_op jit(solution)/shard_map/finish/pallas_call | solution.py:523
  99.0 1.8 %copy.25 = bf16[384,512]{1,0:T(8,128)(2,1)} copy(bf16[384,512]{1,0:T(8,128)(2,1)} %finish.1) | data formatting | bytes 786432
  100.7 0.0 copy-done.8
  100.7 0.6 copy.26
  (5 shorter events, 0.1 us)
Async XLA Ops:
  0.6 22.2 %copy-start = (bf16[768,768]{1,0:T(8,128)(2,1)S(1)}, bf16[768,768]{1,0:T(8,128)(2,1)}, u32[]{:S(2)}) copy-start(bf16[768,768]{1,0:T(8,128)(2,1)} %param.24) | copy-start | bytes 3538948
  2.2 0.6 copy-start.2
  2.2 1.2 %copy-start.4 = (f32[16,384]{1,0:T(8,128)}, f32[16,384]{1,0:T(8,128)S(1)}, u32[]{:S(2)}) copy-start(f32[16,384]{1,0:T(8,128)S(1)} %get-tuple-element.16) | copy-start | bytes 73732
  3.5 19.4 %copy-start.9 = (bf16[3,256]{1,0:T(4,128)(2,1)S(1)}, bf16[3,256]{1,0:T(4,128)(2,1)}, u32[]{:S(2)}) copy-start(bf16[3,256]{1,0:T(4,128)(2,1)} %param.21) | copy-start | bytes 4612
  21.5 56.1 %collective-permute-start = (bf16[2,256]{1,0:T(2,128)(2,1)}, bf16[2,256]{1,0:T(2,128)(2,1)S(1)}, u32[]{:S(2)}, u32[]{:S(2)}) collective-permute-start(bf16[2,256]{1,0:T(2,128)(2,1)} %slice.32), channel_id=1, source_target_pairs={{0,4},{4,8},{8,12},{12,16},{16,20},{20,24},{24,28},{1,5},{5,9},{9,... | collective-permute-start | bytes 3080 | tf_op jit(solution)/shard_map/ppermute | solution.py:513
  24.9 0.9 copy-start.3
  24.9 0.9 copy-start.5
  26.0 1.2 %copy-start.1 = (bf16[8,256,384]{2,1,0:T(8,128)(2,1)}, bf16[8,256,384]{2,1,0:T(8,128)(2,1)S(1)}, u32[]{:S(2)}) copy-start(bf16[8,256,384]{2,1,0:T(8,128)(2,1)S(1)} %broadcast_dynamic-update-slice_fusion.qt) | copy-start | bytes 4718596
  26.0 51.6 %copy-start.6 = (bf16[384,256]{1,0:T(8,128)(2,1)S(1)}, bf16[384,256]{1,0:T(8,128)(2,1)}, u32[]{:S(2)}) copy-start(bf16[384,256]{1,0:T(8,128)(2,1)} %get-tuple-element.12) | copy-start | bytes 589828
  26.0 51.6 %copy-start.7 = (bf16[384,256]{1,0:T(8,128)(2,1)S(1)}, bf16[384,256]{1,0:T(8,128)(2,1)}, u32[]{:S(2)}) copy-start(bf16[384,256]{1,0:T(8,128)(2,1)} %get-tuple-element.11) | copy-start | bytes 589828
  78.5 22.3 %copy-start.8 = (f32[8,384]{1,0:T(8,128)S(1)}, f32[8,384]{1,0:T(8,128)}, u32[]{:S(2)}) copy-start(f32[8,384]{1,0:T(8,128)} %get-tuple-element.25) | copy-start | bytes 36868
where the time goes:
time: 102 us; the launch traced here: 101 us
  Pallas kernels  87.7 us (86%)
  local copies, waits for them, and re-layouts  7.29 us (7%)
  other arithmetic  2.51 us (2%)
  matrix products  1.69 us (2%)
  starting transfers between devices  1.28 us (1%)
    pallas_call x1, Pallas kernels, body(): pl.pallas_call(functools.partial(attend_kernel, nz, nx, ntp, heads), out_...  50.4 us
    pallas_call x1, Pallas kernels, body(): pl.pallas_call(functools.partial(finish_kernel, ntp, chunk), out_shape=st...  20.5 us
    pallas_call x1, Pallas kernels, body(): pl.pallas_call(functools.partial(project_kernel, ntp, chunk), out_shape=[...  16.8 us
    unnamed x24, local copies, waits for them, and re-layouts  4.24 us
  transfers between devices with their start and end apart: 1, of which 0 were waited for; matrix products, arithmetic and copies ran while one was open for 3% of the time, Pallas kernels for 50%

commit v1 on v0

v1 whole, which is shorter than its diff:
```python
import functools
import math

import jax
import jax.numpy as jnp
import numpy as np
from jax import lax
from jax.experimental import pallas as pl
from jax.experimental.pallas import tpu as pltpu
from jax.sharding import PartitionSpec as P

NOPE = 64
ROPE = 32
VDIM = 64
TAPS = 3
LANES = 128
HALO = 16
TURN = 8
AHEAD = 2
WAVE = 2

EPSILON = 1e-06
THETA = 500000.0
NEGATIVE = -1e30
MESH = pl.DeviceIdType.MESH
BF = jnp.bfloat16
F32 = jnp.float32


def remote(src, dst, send, recv, **where):
    return pltpu.make_async_remote_copy(
        src_ref=src, dst_ref=dst, send_sem=send, recv_sem=recv, device_id=where, device_id_type=MESH
    )


def dot(a, b):
    return jnp.dot(a, b, preferred_element_type=F32)


def dot_nt(a, b):
    return lax.dot_general(a, b, (((1,), (1,)), ((), ())), preferred_element_type=F32)


def layer_kernel(
    nz, nx, n, chunk, heads,
    tok, pre, qg, kg, gain, taps, table, wo, wi, ws, wq, wk, wr, wu, wkv, wa, wc,
    out, logs,
    buf, vo, vi, vs, vq, vk, vr, vu, vkv, va, vc, angle,
    vut, upk, upvt, qt, kvs, kn, turn, vt, sbuf, acc, top, low,
    outer, ext, tail, halo, att,
    away, mine, pin, ysend, yin, peer, pown, total, sq, sqin,
    t_s, w_s, own_s, own_r, y_s, y_r, f_s, f_r,
    z_s, o_s, x_s, i_r, d_s, d_r, h_s, h_r,
    a_s, a_r, b_s, b_r, p_s, p_r, q_s, q_r,
):
    sp, tp = lax.axis_index("sp"), lax.axis_index("tp")
    nsp = nz * nx
    z, x = sp // nx, lax.rem(sp, nx)
    ny = n // 2
    y, core = tp // 2, lax.rem(tp, 2)
    partner = tp + 1 - 2 * core
    rows, width = tok.shape
    count = rows // chunk
    pairs = heads // 2
    rank = wkv.shape[0]
    factor2 = (NOPE + ROPE) ** (-0.5) * math.log2(math.e)
    side = pl.ds(pl.multiple_of(core * (rank // 2), LANES), rank // 2)

    def part(r):
        return pl.ds(r * chunk, chunk)

    tokens = [
        pltpu.make_async_copy(tok.at[part(r)], buf.at[tp, part(r)], t_s.at[r]) for r in range(count)
    ]
    place = pl.ds(pl.multiple_of(sp * rows, LANES), rows)
    pairs_of = (
        (wu, vu), (wkv, vkv), (table.at[:, place], angle), (wk, vk), (wr, vr), (wq, vq),
        (wi, vi), (ws, vs), (wo, vo), (wa, va), (wc, vc),
    )
    loads = [pltpu.make_async_copy(a, b, w_s.at[i]) for i, (a, b) in enumerate(pairs_of)]
    for token in tokens:
        token.start()

    barrier = pltpu.get_barrier_semaphore()

    def greet(**where):
        pl.semaphore_signal(barrier, inc=1, device_id=where, device_id_type=MESH)

    for step in range(1, n):
        greet(tp=lax.rem(tp + step, n))
    for step in range(1, nz):
        greet(sp=lax.rem(z + step, nz) * nx + x)
    for step in range(1, nx):
        greet(sp=z * nx + lax.rem(x + step, nx))
    greet(sp=lax.rem(sp + 1, nsp))
    greet(sp=lax.rem(sp + nsp - 1, nsp))
    for load in loads:
        load.start()
    pl.semaphore_wait(barrier, n - 1 + nz - 1 + nx - 1 + 2)

    def y_copy(r, step):
        to = lax.rem(y + step, ny) * 2 + core
        here = buf.at[tp, part(r)]
        return remote(here, here, y_s.at[r, step], y_r.at[r, y], tp=to)

    def y_arrival(r, other):
        here = buf.at[other * 2 + core, part(r)]
        return remote(here, here, y_s.at[r, 0], y_r.at[r, other], tp=partner)

    def own_copy(r):
        here = buf.at[tp, part(r)]
        return remote(here, here, own_s.at[r], own_r.at[r], tp=partner)

    def own_arrival(r):
        here = buf.at[partner, part(r)]
        return remote(here, here, own_s.at[r], own_r.at[r], tp=partner)

    def forward(r, other):
        here = buf.at[other * 2 + core, part(r)]
        return remote(here, here, f_s.at[r, other], f_r.at[r, other], tp=partner)

    def forward_arrival(r, other):
        here = buf.at[other * 2 + 1 - core, part(r)]
        return remote(here, here, f_s.at[r, other], f_r.at[r, other], tp=partner)

    def piece(src, r):
        return kvs.at[src, r, :, side]

    def column_copy(r, k):
        return remote(piece(sp, r), piece(sp, r), z_s.at[r, k], i_r.at[sp, r], sp=sp + k * nx)

    def own_side(r, step):
        to = z * nx + lax.rem(x + step, nx)
        return remote(piece(sp, r), piece(sp, r), o_s.at[r, step], i_r.at[sp, r], sp=to)

    def relay(k, r, step):
        src = sp - k * nx
        to = z * nx + lax.rem(x + step, nx)
        return remote(piece(src, r), piece(src, r), x_s.at[k, r, step], i_r.at[src, r], sp=to)

    def arrival(src, r):
        return remote(piece(src, r), piece(src, r), z_s.at[r, 0], i_r.at[src, r], tp=partner)

    def share(src, r):
        return remote(piece(src, r), piece(src, r), d_s.at[src, r], d_r.at[src, r], tp=partner)

    def share_arrival(src, r):
        other = pl.ds(pl.multiple_of((1 - core) * (rank // 2), LANES), rank // 2)
        here = kvs.at[src, r, :, other]
        return remote(here, here, d_s.at[src, r], d_r.at[src, r], tp=partner)

    def halo_copy():
        return remote(tail, halo, h_s.at[0], h_r.at[0], sp=sp + 1)

    for r in range(count):
        tokens[r].wait()
        for step in range(1, ny):
            y_copy(r, step).start()
        own_copy(r).start()

    qt[...] = jnp.zeros_like(qt)
    loads[0].wait()
    vut[...] = vu[...].T
    loads[1].wait()
    for p in range(pairs):
        first, second = 2 * p * LANES, (2 * p + 1) * LANES
        upk[:, p * LANES : (p + 1) * LANES] = jnp.concatenate(
            [vkv[:, first : first + NOPE], vkv[:, second : second + NOPE]], axis=1
        )
    turned = vkv[...].T
    for h in range(heads):
        upvt[h * VDIM : (h + 1) * VDIM] = turned[h * LANES + NOPE : (h + 1) * LANES]

    def raise_keys(src, slot, span):
        count_here = len(span)
        lat = jnp.concatenate([kvs[src, r, : chunk] for r in span], axis=0)
        here = pl.ds(span[0] * chunk, count_here * chunk)
        kn[slot, here] = dot(lat, upk[...]).astype(BF)
        vt[slot, :, here] = dot_nt(upvt[...], lat).astype(BF)
        for r in span:
            packed = kvs[src, r, chunk:].astype(F32)
            tall = jnp.concatenate(
                [packed[:, g * LANES : (g + 1) * LANES] for g in range(ROPE // TURN)]
                + [jnp.zeros((LANES - ROPE, LANES), F32)],
                axis=0,
            )
            turn[slot, part(r)] = tall.T.astype(BF)

    def units(todo, slot, diagonal):
        peaks, ready = {}, {}
        size = len(todo)

        def keys(c):
            return (c + 1) * chunk if diagonal else rows

        def score(i):
            c, p = todo[i]
            k = keys(c)
            left = jnp.concatenate(
                [kn[slot, :k, p * LANES : (p + 1) * LANES], turn[slot, :k]], axis=1
            )
            s = dot(left, qt[c, p])
            if diagonal:
                last = s[k - chunk :]
                key = lax.broadcasted_iota(jnp.int32, last.shape, 0)
                query = lax.rem(lax.broadcasted_iota(jnp.int32, last.shape, 1), chunk)
                last = jnp.where(key <= query, last, NEGATIVE)
                s = last if k == chunk else jnp.concatenate([s[: k - chunk], last], axis=0)
            sbuf[i % (AHEAD + 2), :k] = s
            peaks[i] = jnp.max(s, axis=0, keepdims=True) * factor2

        def soften(i):
            c, p = todo[i]
            peak = peaks.pop(i)
            shrink = None
            if not diagonal:
                before = top[c, p]
                peak = jnp.maximum(before, peak)
                shrink = jnp.exp2(before - peak)
            w = jnp.exp2(sbuf[i % (AHEAD + 2), : keys(c)] * factor2 - peak)
            sums = jnp.sum(w, axis=0, keepdims=True)
            low[c, p] = sums if diagonal else low[c, p] * shrink + sums
            top[c, p] = peak
            ready[i] = (w.astype(BF), shrink)

        def gather(i):
            c, p = todo[i]
            w, shrink = ready.pop(i)
            o = dot(vt[slot, p * LANES : (p + 1) * LANES, : keys(c)], w)
            o = jnp.concatenate([o[:VDIM, :chunk], o[VDIM:, chunk:]], axis=1)
            acc[c, p] = o if diagonal else acc[c, p] * shrink + o

        for t in range(size + AHEAD + 1):
            if t < size:
                score(t)
            if 0 <= t - AHEAD < size:
                soften(t - AHEAD)
            if 0 <= t - AHEAD - 1 < size:
                gather(t - AHEAD - 1)

    def project(r):
        for step in range(1, ny):
            other = lax.rem(y + ny - step, ny)
            y_arrival(r, other).wait_recv()
            forward(r, other).start()
        own_arrival(r).wait_recv()
        for step in range(1, ny):
            forward_arrival(r, lax.rem(y + ny - step, ny)).wait_recv()
        if r == 0:
            for load in loads[2:5]:
                load.wait()
        here = part(r)
        wide = jnp.concatenate([buf[s, here] for s in range(n)], axis=1).astype(F32)
        factor = lax.rsqrt(jnp.sum(wide * wide, axis=1, keepdims=True) / (n * width) + EPSILON)
        scaled = (wide * pre[...]).astype(BF)
        flat = jnp.broadcast_to(factor, (chunk, LANES)).T[:1]
        cosine, sine = angle[: ROPE // 2, here], angle[ROPE // 2 :, here]

        def rotate(first, second):
            return jnp.concatenate(
                [first * cosine - second * sine, second * cosine + first * sine], axis=0
            )

        kv = dot(scaled, vk[...]) * factor
        kv = kv * lax.rsqrt(jnp.mean(kv * kv, axis=1, keepdims=True) + EPSILON) * kg[...]
        kvs[sp, r, :chunk] = kv.astype(BF)
        key = dot_nt(vr[...], scaled) * flat
        key = rotate(key[: ROPE // 2], key[ROPE // 2 :])
        kvs[sp, r, chunk:] = jnp.concatenate(
            [key[g * TURN : (g + 1) * TURN] for g in range(ROPE // TURN)], axis=1
        ).astype(BF)
        for k in range(1, nz):
            @pl.when(z + k < nz)
            def _(k=k):
                column_copy(r, k).start()
        for step in range(1, nx):
            @pl.when(x + step < nx)
            def _(step=step):
                own_side(r, step).start()

        if r == 0:
            loads[5].wait()
        q = dot(scaled, vq[...]) * factor
        gains = jnp.concatenate([qg[i : i + 1] for i in range(qg.shape[0])], axis=1)
        q = q * lax.rsqrt(jnp.mean(q * q, axis=1, keepdims=True) + EPSILON) * gains
        query = dot_nt(vut[...], q.astype(BF))
        for h in range(heads):
            p, low_half = h // 2, h % 2
            base = h * (NOPE + ROPE)
            span = slice(low_half * chunk, (low_half + 1) * chunk)
            qt[r, p, low_half * NOPE : (low_half + 1) * NOPE, span] = query[
                base : base + NOPE
            ].astype(BF)
            middle = base + NOPE + ROPE // 2
            qt[r, p, 2 * NOPE : 2 * NOPE + ROPE, span] = rotate(
                query[base + NOPE : middle], query[middle : base + NOPE + ROPE]
            ).astype(BF)

        if r == 0:
            for load in loads[6:9]:
                load.wait()
        inner = (dot(scaled, vi[...]) * factor).astype(BF).astype(F32)
        source = (dot(scaled, vs[...]) * factor).astype(BF).astype(F32)
        driven = (inner * source).astype(BF)
        ext[8 + r * chunk : 8 + (r + 1) * chunk] = driven.astype(F32)
        if r == count - 1:
            tail[...] = driven[chunk - HALO :]

            @pl.when(sp < nsp - 1)
            def _():
                halo_copy().start()
        outer[here] = (dot(scaled, vo[...]) * factor).astype(BF)
        raise_keys(sp, 0, [r])
        units([(r, p) for p in range(pairs)], 0, True)

    for r in range(count):
        project(r)

    items = z * nx + x

    def place_of(i):
        j = i - x
        level = jnp.where(j < 0, 0, j // nx + 1)
        turn_of = lax.rem(j + nx, nx)
        across_x = jnp.where(j < 0, i, lax.rem(x + turn_of, nx))
        column = jnp.logical_and(j >= 0, turn_of == 0)
        level = jnp.where(column, level, jnp.where(j < 0, 0, level))
        return (z - level) * nx + across_x, level, column

    def fetch(i):
        src, level, column = place_of(i)
        for r in range(count):
            arrival(src, r).wait_recv()
            share(src, r).start()

            @pl.when(column)
            def _(r=r):
                for step in range(1, nx):
                    relay(level, r, step).start()

    def take(i, slot):
        src, _, _ = place_of(i)
        for r in range(count):
            share_arrival(src, r).wait_recv()
        raise_keys(src, slot, list(range(count)))

    wave = jnp.minimum(items, WAVE)

    def whole(i, carry):
        fetch(i)
        take(i, 0)
        units([(c, p) for c in range(count) for p in range(pairs)], 0, False)
        return carry

    lax.fori_loop(0, items - wave, whole, 0)

    def ready(w, carry):
        fetch(items - wave + w)
        take(items - wave + w, w)
        return carry

    lax.fori_loop(0, wave, ready, 0)

    @pl.when(sp == 0)
    def _():
        ext[:8] = jnp.zeros((8, ext.shape[1]), F32)

    @pl.when(sp > 0)
    def _():
        remote(tail, halo, h_s.at[0], h_r.at[0], tp=partner).wait_recv()
        ext[:8] = halo[...].astype(F32)[HALO - 8 :]

    def product(r, dest):
        columns = pl.ds(pl.multiple_of(dest * width, width), width)
        return (
            dot(att[part(r), : heads * VDIM], va[:, columns])
            + dot(att[part(r), heads * VDIM :], vc[:, columns])
        ).astype(BF)

    def to_partner(r, step):
        return remote(
            away.at[step, part(r)], pin.at[step, part(r)], a_s.at[r, step], a_r.at[r, step], tp=partner
        )

    def across(r, step):
        to = lax.rem(y + step, ny) * 2 + core
        return remote(
            ysend.at[step, part(r)], yin.at[step, part(r)], b_s.at[r, step], b_r.at[r, step], tp=to
        )

    def home(r):
        return remote(peer.at[part(r)], pown.at[part(r)], p_s.at[r], p_r.at[r], tp=partner)

    def squares(r, step):
        return remote(
            sq.at[r], sqin.at[step, r], q_s.at[r, step], q_r.at[r, step], tp=lax.rem(tp + step, n)
        )

    for load in loads[9:]:
        load.wait()

    for c in range(count):
        def last(w, carry, c=c):
            units([(c, p) for p in range(pairs)], w, False)
            return carry

        lax.fori_loop(0, wave, last, 0)
        for p in range(pairs):
            value = acc[c, p] / low[c, p]
            both = jnp.concatenate([value[:, :chunk], value[:, chunk:]], axis=0)
            att[part(c), p * LANES : (p + 1) * LANES] = both.T.astype(BF)
            log = top[c, p] * math.log(2.0) + jnp.log(low[c, p])
            logs[2 * p : 2 * p + 1, part(c)] = log[:, :chunk]
            logs[2 * p + 1 : 2 * p + 2, part(c)] = log[:, chunk:]
        conv = jnp.zeros((chunk, ext.shape[1]), F32)
        for index in range(TAPS):
            start = 8 + c * chunk - (TAPS - 1) + index
            conv = conv + taps[index : index + 1].astype(F32) * ext[start : start + chunk]
        att[part(c), heads * VDIM :] = (outer[part(c)].astype(F32) * conv).astype(BF)
        for step in range(1, ny):
            dest = lax.rem(y + step, ny) * 2
            away[step, part(c)] = product(c, dest + 1 - core)
            to_partner(c, step).start()
            mine[step, part(c)] = product(c, dest + core)
        peer[part(c)] = product(c, partner)
        home(c).start()
        for step in range(1, ny):
            to_partner(c, step).wait_recv()
            ysend[step, part(c)] = (
                mine[step, part(c)].astype(F32) + pin[step, part(c)].astype(F32)
            ).astype(BF)
            across(c, step).start()
        total[part(c)] = product(c, tp).astype(F32)
    for r in range(count):
        home(r).wait_recv()
        value = total[part(r)] + pown[part(r)].astype(F32)
        for step in range(1, ny):
            across(r, step).wait_recv()
            value = value + yin[step, part(r)].astype(F32)
        total[part(r)] = value
        sums = jnp.sum(value * value, axis=1, keepdims=True)
        sq[r] = jnp.broadcast_to(sums, (chunk, LANES)).T[:8]
        for step in range(1, n):
            squares(r, step).start()
    for r in range(count):
        whole_sum = sq[r]
        for step in range(1, n):
            squares(r, step).wait_recv()
            whole_sum = whole_sum + sqin[step, r]
        scale = lax.rsqrt(whole_sum / (n * width) + EPSILON)
        column = jnp.broadcast_to(scale[:1], (LANES, chunk)).T[:, :1]
        out[part(r)] = (total[part(r)] * column * gain[...]).astype(BF)

    for r in range(count):
        own_copy(r).wait_send()
        home(r).wait_send()
        for step in range(1, ny):
            y_copy(r, step).wait_send()
            forward(r, lax.rem(y + step, ny)).wait_send()
            to_partner(r, step).wait_send()
            across(r, step).wait_send()
        for step in range(1, n):
            squares(r, step).wait_send()
        for k in range(1, nz):
            @pl.when(z + k < nz)
            def _(k=k, r=r):
                column_copy(r, k).wait_send()
        for step in range(1, nx):
            @pl.when(x + step < nx)
            def _(step=step, r=r):
                own_side(r, step).wait_send()

    @pl.when(sp < nsp - 1)
    def _():
        halo_copy().wait_send()

    def sent(i, carry):
        src, level, column = place_of(i)
        for r in range(count):
            share(src, r).wait_send()

            @pl.when(column)
            def _(r=r):
                for step in range(1, nx):
                    relay(level, r, step).wait_send()
        return carry

    lax.fori_loop(0, items, sent, 0)


DMA = pltpu.SemaphoreType.DMA


def angles(tokens):
    freqs = np.float32(THETA) ** (-np.arange(0, ROPE, 2, dtype=np.float32) / np.float32(ROPE))
    phase = freqs.astype(np.float32)[:, None] * np.arange(tokens, dtype=np.float32)[None, :]
    phase = phase.astype(np.float64)
    return np.concatenate([np.cos(phase), np.sin(phase)], axis=0).astype(np.float32)


def body(
    nsp, ntp,
    tokens, pre_gain, outer_gate_weight, inner_gate_weight, source_weight, conv_taps,
    q_down_weight, q_norm_gain, q_up_weight, kv_down_weight, rope_key_weight, kv_norm_gain,
    kv_up_weight, attn_out_weight, conv_out_weight, post_gain,
):
    rows, width = tokens.shape
    ny = ntp // 2
    nx = ny if nsp % ny == 0 else 1
    nz = nsp // nx
    chunk = LANES
    count = rows // chunk
    q_rank, rank = q_down_weight.shape[1], kv_down_weight.shape[1]
    channels = outer_gate_weight.shape[1]
    heads = q_up_weight.shape[1] // (NOPE + ROPE)
    pairs = heads // 2
    struct = jax.ShapeDtypeStruct
    v = pltpu.VMEM
    whole = pl.BlockSpec(memory_space=pltpu.VMEM)
    anywhere = pl.BlockSpec(memory_space=pl.ANY)
    rope_turned = rope_key_weight.T
    weights = (
        outer_gate_weight, inner_gate_weight, source_weight, q_down_weight, kv_down_weight,
        rope_turned, q_up_weight, kv_up_weight, attn_out_weight, conv_out_weight,
    )
    block = (ny, rows, width)
    return pl.pallas_call(
        functools.partial(layer_kernel, nz, nx, ntp, chunk, heads),
        out_shape=[struct((rows, width), BF), struct((heads, rows), F32)],
        in_specs=[anywhere] + [whole] * 5 + [anywhere] * (1 + len(weights)),
        out_specs=[whole] * 2,
        scratch_shapes=[v((ntp, rows, width), BF)]
        + [v(w.shape, BF) for w in weights]
        + [
            v((ROPE, rows), F32),
            v(q_up_weight.shape[::-1], BF),
            v((rank, heads * NOPE), BF), v((heads * VDIM, rank), BF),
            v((count, pairs, 2 * LANES, 2 * chunk), BF),
            v((nsp, count, chunk + TURN, rank), BF),
            v((WAVE, rows, heads * NOPE), BF), v((WAVE, rows, LANES), BF),
            v((WAVE, heads * VDIM, rows), BF),
            v((AHEAD + 2, rows, 2 * chunk), F32),
            v((count, pairs, VDIM, 2 * chunk), F32),
            v((count, pairs, 1, 2 * chunk), F32), v((count, pairs, 1, 2 * chunk), F32),
            v((rows, channels), BF), v((8 + rows, channels), F32),
            v((HALO, channels), BF), v((HALO, channels), BF),
            v((rows, heads * VDIM + channels), BF),
        ]
        + [v(block, BF)] * 5
        + [
            v((rows, width), BF), v((rows, width), BF), v((rows, width), F32),
            v((count, 8, chunk), F32), v((ntp, count, 8, chunk), F32),
            DMA((count,)), DMA((11,)), DMA((count,)), DMA((count,)),
            DMA((count, ny)), DMA((count, ny)), DMA((count, ny)), DMA((count, ny)),
            DMA((count, nz)), DMA((count, nx)), DMA((nz, count, nx)),
            DMA((nsp, count)), DMA((nsp, count)), DMA((nsp, count)), DMA((1,)), DMA((1,)),
            DMA((count, ny)), DMA((count, ny)), DMA((count, ny)), DMA((count, ny)),
            DMA((count,)), DMA((count,)), DMA((count, ntp)), DMA((count, ntp)),
        ],
        compiler_params=pltpu.CompilerParams(
            collective_id=0, has_side_effects=True, vmem_limit_bytes=60 * 1024 * 1024
        ),
        name="layer",
    )(
        tokens, pre_gain[None], q_norm_gain.reshape(-1, LANES), kv_norm_gain[None],
        post_gain[None], conv_taps, jnp.asarray(angles(nsp * rows)), *weights,
    )


def solution(mesh):
    placed = (
        P("sp", "tp"), P(), P(None, "tp"), P(None, "tp"), P(None, "tp"), P(None, "tp"), P(), P(),
        P(None, "tp"), P(), P(), P(), P(None, "tp"), P("tp", None), P("tp", None), P("tp"),
    )
    return jax.shard_map(
        functools.partial(body, mesh.shape["sp"], mesh.shape["tp"]),
        mesh=mesh,
        in_specs=placed,
        out_specs=(P("sp", "tp"), P("tp", "sp")),
        check_vma=False,
    )
```

time: 102 us -> 74.4 us (0.73)
  the two profiles are of different devices: /device:TPU:27 before, /device:TPU:25 now
where the time goes in v1:
time: 74.4 us; the launch traced here: 74.2 us
  Pallas kernels  70.4 us (95%)
  local copies, waits for them, and re-layouts  3.07 us (4%)
    pallas_call x1, Pallas kernels, body(): pl.pallas_call(functools.partial(layer_kernel, nz, nx, ntp, chunk, heads)...  70.4 us
    unnamed x2, local copies, waits for them, and re-layouts  3.07 us

profile of v1, /device:TPU:25, one launch (start us, length us, event | category | flops | bytes accessed | tf_op | source)
XLA Modules:
  0.0 74.2 jit_solution(2720292412058248829)
XLA Ops:
  0.6 70.4 %layer.1 = (bf16[384,512]{1,0:T(8,128)(2,1)}, f32[8,384]{1,0:T(8,128)}) custom-call(bf16[384,512]{1,0:T(8,128)(2,1)} %tok.1, f32[1,2048]{1,0:T(1,128)} %bitcast.6, f32[6,128]{1,0:T(8,128)} %bitcast.7, f32[1,512]{1,0:T(1,128)} %bitcast.8, f32[1,512]{1,0:T(1,128)} %bitcast.9, bf16[3,256]{1,0:T(4,128)(2,1)} %taps.1, f32[32,3072]{1,0:T(8,128)} %constant.2.clone.table, ...), custom_call_target="tpu_custom_call" | custom-call | tf_op jit(solution)/shard_map/layer/pallas_call | solution.py:527
  71.1 1.8 %copy.21 = bf16[384,512]{1,0:T(8,128)(2,1)} copy(bf16[384,512]{1,0:T(8,128)(2,1)} %get-tuple-element.4) | data formatting | bytes 786432
  72.9 1.3 %copy.22 = f32[8,384]{1,0:T(8,128)} copy(f32[8,384]{1,0:T(8,128)} %get-tuple-element.5) | data formatting | bytes 24576

commit v2 on v1

--- a/solution.py
+++ b/solution.py
@@ -17,7 +17,7 @@
 HALO = 16
 TURN = 8
 AHEAD = 2
-WAVE = 2
+WAVE = 1
 
 EPSILON = 1e-06
 THETA = 500000.0
@@ -96,7 +96,8 @@
     greet(sp=lax.rem(sp + nsp - 1, nsp))
     for load in loads:
         load.start()
-    pl.semaphore_wait(barrier, n - 1 + nz - 1 + nx - 1 + 2)
+    with jax.named_scope("barrier"):
+        pl.semaphore_wait(barrier, n - 1 + nz - 1 + nx - 1 + 2)
 
     def y_copy(r, step):
         to = lax.rem(y + step, ny) * 2 + core
@@ -152,16 +153,19 @@
     def halo_copy():
         return remote(tail, halo, h_s.at[0], h_r.at[0], sp=sp + 1)
 
-    for r in range(count):
-        tokens[r].wait()
-        for step in range(1, ny):
-            y_copy(r, step).start()
-        own_copy(r).start()
-
-    qt[...] = jnp.zeros_like(qt)
-    loads[0].wait()
-    vut[...] = vu[...].T
-    loads[1].wait()
+    with jax.named_scope("sendtok"):
+        for r in range(count):
+            tokens[r].wait()
+            for step in range(1, ny):
+                y_copy(r, step).start()
+            own_copy(r).start()
+
+    with jax.named_scope("wturn"):
+        qt[...] = jnp.zeros_like(qt)
+        loads[0].wait()
+        vut[...] = vu[...].T
+    with jax.named_scope("wload1"):
+        loads[1].wait()
     for p in range(pairs):
         first, second = 2 * p * LANES, (2 * p + 1) * LANES
         upk[:, p * LANES : (p + 1) * LANES] = jnp.concatenate(
@@ -238,17 +242,67 @@
             if 0 <= t - AHEAD - 1 < size:
                 gather(t - AHEAD - 1)
 
-    def project(r):
+    items = z * nx + x
+
+    def place_of(i):
+        j = i - x
+        turn_of = lax.rem(j + nx, nx)
+        across_x = jnp.where(j < 0, i, lax.rem(x + turn_of, nx))
+        level = jnp.where(j < 0, 0, j // nx + 1)
+        column = jnp.logical_and(j >= 0, turn_of == 0)
+        return (z - level) * nx + across_x, column
+
+    def pump(k, r):
+        @pl.when(k <= z)
+        def _():
+            src = sp - k * nx
+            arrival(src, r).wait_recv()
+            share(src, r).start()
+            for step in range(1, nx):
+                relay(k, r, step).start()
+
+    def fetch(i):
+        src, column = place_of(i)
+
+        @pl.when(jnp.logical_and(i < items, jnp.logical_not(column)))
+        def _():
+            for r in range(count):
+                arrival(src, r).wait_recv()
+                share(src, r).start()
+
+    def take(i, slot):
+        src, _ = place_of(i)
+        with jax.named_scope("sharewait"):
+            for r in range(count):
+                share_arrival(src, r).wait_recv()
+        raise_keys(src, slot, list(range(count)))
+        with jax.named_scope("pump"):
+            @pl.when(i > 0)
+            def _():
+                for r in range(count - 1):
+                    pump(i + 2, r)
+
+            pump(i + 2, count - 1)
+        with jax.named_scope("fetch"):
+            fetch(i + 1)
+
+    def pass_on(r):
         for step in range(1, ny):
             other = lax.rem(y + ny - step, ny)
             y_arrival(r, other).wait_recv()
             forward(r, other).start()
-        own_arrival(r).wait_recv()
-        for step in range(1, ny):
-            forward_arrival(r, lax.rem(y + ny - step, ny)).wait_recv()
+
+    def project(r):
+        with jax.named_scope(f"tokwait{r}"):
+            if r == 0:
+                pass_on(r)
+            own_arrival(r).wait_recv()
+            for step in range(1, ny):
+                forward_arrival(r, lax.rem(y + ny - step, ny)).wait_recv()
         if r == 0:
-            for load in loads[2:5]:
-                load.wait()
+            with jax.named_scope("wload2"):
+                for load in loads[2:5]:
+                    load.wait()
         here = part(r)
         wide = jnp.concatenate([buf[s, here] for s in range(n)], axis=1).astype(F32)
         factor = lax.rsqrt(jnp.sum(wide * wide, axis=1, keepdims=True) / (n * width) + EPSILON)
@@ -279,10 +333,18 @@
                 own_side(r, step).start()
 
         if r == 0:
-            loads[5].wait()
+            with jax.named_scope("wload5"):
+                loads[5].wait()
         q = dot(scaled, vq[...]) * factor
         gains = jnp.concatenate([qg[i : i + 1] for i in range(qg.shape[0])], axis=1)
         q = q * lax.rsqrt(jnp.mean(q * q, axis=1, keepdims=True) + EPSILON) * gains
+        with jax.named_scope("passon"):
+            if r + 1 < count:
+                pass_on(r + 1)
+            else:
+                for k in range(1, min(nz, 3)):
+                    for early in range(count - 2):
+                        pump(k, early)
         query = dot_nt(vut[...], q.astype(BF))
         for h in range(heads):
             p, low_half = h // 2, h % 2
@@ -297,8 +359,9 @@
             ).astype(BF)
 
         if r == 0:
-            for load in loads[6:9]:
-                load.wait()
+            with jax.named_scope("wload6"):
+                for load in loads[6:9]:
+                    load.wait()
         inner = (dot(scaled, vi[...]) * factor).astype(BF).astype(F32)
         source = (dot(scaled, vs[...]) * factor).astype(BF).astype(F32)
         driven = (inner * source).astype(BF)
@@ -310,52 +373,30 @@
             def _():
                 halo_copy().start()
         outer[here] = (dot(scaled, vo[...]) * factor).astype(BF)
-        raise_keys(sp, 0, [r])
-        units([(r, p) for p in range(pairs)], 0, True)
+        if r == count - 1:
+            with jax.named_scope("prefetch"):
+                for k in range(1, min(nz, 3)):
+                    pump(k, count - 2)
+                fetch(0)
+                pump(1, count - 1)
+        with jax.named_scope(f"diag{r}"):
+            raise_keys(sp, 0, [r])
+            units([(r, p) for p in range(pairs)], 0, True)
 
     for r in range(count):
         project(r)
 
-    items = z * nx + x
-
-    def place_of(i):
-        j = i - x
-        level = jnp.where(j < 0, 0, j // nx + 1)
-        turn_of = lax.rem(j + nx, nx)
-        across_x = jnp.where(j < 0, i, lax.rem(x + turn_of, nx))
-        column = jnp.logical_and(j >= 0, turn_of == 0)
-        level = jnp.where(column, level, jnp.where(j < 0, 0, level))
-        return (z - level) * nx + across_x, level, column
-
-    def fetch(i):
-        src, level, column = place_of(i)
-        for r in range(count):
-            arrival(src, r).wait_recv()
-            share(src, r).start()
-
-            @pl.when(column)
-            def _(r=r):
-                for step in range(1, nx):
-                    relay(level, r, step).start()
-
-    def take(i, slot):
-        src, _, _ = place_of(i)
-        for r in range(count):
-            share_arrival(src, r).wait_recv()
-        raise_keys(src, slot, list(range(count)))
-
     wave = jnp.minimum(items, WAVE)
 
     def whole(i, carry):
-        fetch(i)
         take(i, 0)
-        units([(c, p) for c in range(count) for p in range(pairs)], 0, False)
+        with jax.named_scope("units"):
+          units([(c, p) for c in range(count) for p in range(pairs)], 0, False)
         return carry
 
     lax.fori_loop(0, items - wave, whole, 0)
 
     def ready(w, carry):
-        fetch(items - wave + w)
         take(items - wave + w, w)
         return carry
 
@@ -399,12 +440,24 @@
     for load in loads[9:]:
         load.wait()
 
+    def send_on(c):
+        for step in range(1, ny):
+            with jax.named_scope("partnerwait"):
+                to_partner(c, step).wait_recv()
+            ysend[step, part(c)] = (
+                mine[step, part(c)].astype(F32) + pin[step, part(c)].astype(F32)
+            ).astype(BF)
+            across(c, step).start()
+
     for c in range(count):
         def last(w, carry, c=c):
-            units([(c, p) for p in range(pairs)], w, False)
+            with jax.named_scope("lastunits"):
+                units([(c, p) for p in range(pairs)], w, False)
             return carry
 
         lax.fori_loop(0, wave, last, 0)
+        if c > 0:
+            send_on(c - 1)
         for p in range(pairs):
             value = acc[c, p] / low[c, p]
             both = jnp.concatenate([value[:, :chunk], value[:, chunk:]], axis=0)
@@ -424,18 +477,16 @@
             mine[step, part(c)] = product(c, dest + core)
         peer[part(c)] = product(c, partner)
         home(c).start()
-        for step in range(1, ny):
-            to_partner(c, step).wait_recv()
-            ysend[step, part(c)] = (
-                mine[step, part(c)].astype(F32) + pin[step, part(c)].astype(F32)
-            ).astype(BF)
-            across(c, step).start()
         total[part(c)] = product(c, tp).astype(F32)
+        if c == count - 1:
+            send_on(c)
     for r in range(count):
-        home(r).wait_recv()
+        with jax.named_scope("homewait"):
+            home(r).wait_recv()
         value = total[part(r)] + pown[part(r)].astype(F32)
         for step in range(1, ny):
-            across(r, step).wait_recv()
+            with jax.named_scope("acrosswait"):
+                across(r, step).wait_recv()
             value = value + yin[step, part(r)].astype(F32)
         total[part(r)] = value
         sums = jnp.sum(value * value, axis=1, keepdims=True)
@@ -445,14 +496,18 @@
     for r in range(count):
         whole_sum = sq[r]
         for step in range(1, n):
-            squares(r, step).wait_recv()
+            with jax.named_scope("sqwait"):
+                squares(r, step).wait_recv()
             whole_sum = whole_sum + sqin[step, r]
         scale = lax.rsqrt(whole_sum / (n * width) + EPSILON)
         column = jnp.broadcast_to(scale[:1], (LANES, chunk)).T[:, :1]
         out[part(r)] = (total[part(r)] * column * gain[...]).astype(BF)
 
+    with jax.named_scope("endsends"):
+        own_copy(0).wait_send()
     for r in range(count):
-        own_copy(r).wait_send()
+        if r > 0:
+            own_copy(r).wait_send()
         home(r).wait_send()
         for step in range(1, ny):
             y_copy(r, step).wait_send()
@@ -475,17 +530,20 @@
         halo_copy().wait_send()
 
     def sent(i, carry):
-        src, level, column = place_of(i)
+        src, _ = place_of(i)
         for r in range(count):
             share(src, r).wait_send()
-
-            @pl.when(column)
-            def _(r=r):
-                for step in range(1, nx):
-                    relay(level, r, step).wait_send()
         return carry
 
     lax.fori_loop(0, items, sent, 0)
+
+    def relayed(k, carry):
+        for r in range(count):
+            for step in range(1, nx):
+                relay(k, r, step).wait_send()
+        return carry
+
+    lax.fori_loop(1, z + 1, relayed, 0)
 
 
 DMA = pltpu.SemaphoreType.DMA
@@ -526,7 +584,7 @@
     block = (ny, rows, width)
     return pl.pallas_call(
         functools.partial(layer_kernel, nz, nx, ntp, chunk, heads),
-        out_shape=[struct((rows, width), BF), struct((heads, rows), F32)],
+        out_shape=[v((rows, width), BF), v((heads, rows), F32)],
         in_specs=[anywhere] + [whole] * 5 + [anywhere] * (1 + len(weights)),
         out_specs=[whole] * 2,
         scratch_shapes=[v((ntp, rows, width), BF)]

time: 74.4 us -> 64.2 us (0.86)
  the two profiles are of different devices: /device:TPU:25 before, /device:TPU:27 now
where the time goes in v2:
time: 64.2 us; the launch traced here: 64 us
  Pallas kernels  62 us (97%)
  local copies, waits for them, and re-layouts  1.35 us (2%)
  between operations  0.65 us (1%)
    pallas_call x1, Pallas kernels, body(): pl.pallas_call(functools.partial(layer_kernel, nz, nx, ntp, chunk, heads)...  62 us
    unnamed x2, local copies, waits for them, and re-layouts  1.35 us

profile of v2, /device:TPU:27, one launch (start us, length us, event | category | flops | bytes accessed | tf_op | source)
XLA Modules:
  0.0 64.0 jit_solution(6361270974839637744)
XLA Ops:
  0.6 62.0 %layer.1 = (bf16[384,512]{1,0:T(8,128)(2,1)S(1)}, f32[8,384]{1,0:T(8,128)S(1)}) custom-call(bf16[384,512]{1,0:T(8,128)(2,1)} %tok.1, f32[1,2048]{1,0:T(1,128)} %bitcast.6, f32[6,128]{1,0:T(8,128)} %bitcast.7, f32[1,512]{1,0:T(1,128)} %bitcast.8, f32[1,512]{1,0:T(1,128)} %bitcast.9, bf16[3,256]{1,0:T(4,128)(2,1)} %taps.1, f32[32,3072]{1,0:T(8,128)} %constant.2.clone.table, ...), custom_call_target="tpu_custom_call" | custom-call | tf_op jit(solution)/shard_map/layer/pallas_call | solution.py:585
  62.7 0.7 %copy.21 = bf16[384,512]{1,0:T(8,128)(2,1)} copy(bf16[384,512]{1,0:T(8,128)(2,1)S(1)} %get-tuple-element.2) | data formatting | bytes 786432
  63.4 0.6 copy.22

commit v3 on v2

--- a/solution.py
+++ b/solution.py
@@ -17,7 +17,7 @@
 HALO = 16
 TURN = 8
 AHEAD = 2
-WAVE = 1
+WAVE = 3
 
 EPSILON = 1e-06
 THETA = 500000.0
@@ -47,7 +47,7 @@
     out, logs,
     buf, vo, vi, vs, vq, vk, vr, vu, vkv, va, vc, angle,
     vut, upk, upvt, qt, kvs, kn, turn, vt, sbuf, acc, top, low,
-    outer, ext, tail, halo, att,
+    scale_of, factors, outer, ext, tail, halo, att,
     away, mine, pin, ysend, yin, peer, pown, total, sq, sqin,
     t_s, w_s, own_s, own_r, y_s, y_r, f_s, f_r,
     z_s, o_s, x_s, i_r, d_s, d_r, h_s, h_r,
@@ -88,8 +88,8 @@
 
     for step in range(1, n):
         greet(tp=lax.rem(tp + step, n))
-    for step in range(1, nz):
-        greet(sp=lax.rem(z + step, nz) * nx + x)
+    greet(sp=lax.rem(z + 1, nz) * nx + x)
+    greet(sp=lax.rem(z + nz - 1, nz) * nx + x)
     for step in range(1, nx):
         greet(sp=z * nx + lax.rem(x + step, nx))
     greet(sp=lax.rem(sp + 1, nsp))
@@ -97,7 +97,7 @@
     for load in loads:
         load.start()
     with jax.named_scope("barrier"):
-        pl.semaphore_wait(barrier, n - 1 + nz - 1 + nx - 1 + 2)
+        pl.semaphore_wait(barrier, n - 1 + 2 + nx - 1 + 2)
 
     def y_copy(r, step):
         to = lax.rem(y + step, ny) * 2 + core
@@ -127,8 +127,9 @@
     def piece(src, r):
         return kvs.at[src, r, :, side]
 
-    def column_copy(r, k):
-        return remote(piece(sp, r), piece(sp, r), z_s.at[r, k], i_r.at[sp, r], sp=sp + k * nx)
+    def up_copy(k, r):
+        src = sp - k * nx
+        return remote(piece(src, r), piece(src, r), z_s.at[k, r], i_r.at[src, r], sp=sp + nx)
 
     def own_side(r, step):
         to = z * nx + lax.rem(x + step, nx)
@@ -140,7 +141,7 @@
         return remote(piece(src, r), piece(src, r), x_s.at[k, r, step], i_r.at[src, r], sp=to)
 
     def arrival(src, r):
-        return remote(piece(src, r), piece(src, r), z_s.at[r, 0], i_r.at[src, r], tp=partner)
+        return remote(piece(src, r), piece(src, r), z_s.at[0, r], i_r.at[src, r], tp=partner)
 
     def share(src, r):
         return remote(piece(src, r), piece(src, r), d_s.at[src, r], d_r.at[src, r], tp=partner)
@@ -190,7 +191,7 @@
             )
             turn[slot, part(r)] = tall.T.astype(BF)
 
-    def units(todo, slot, diagonal):
+    def units(todo, diagonal):
         peaks, ready = {}, {}
         size = len(todo)
 
@@ -198,7 +199,7 @@
             return (c + 1) * chunk if diagonal else rows
 
         def score(i):
-            c, p = todo[i]
+            c, p, slot = todo[i]
             k = keys(c)
             left = jnp.concatenate(
                 [kn[slot, :k, p * LANES : (p + 1) * LANES], turn[slot, :k]], axis=1
@@ -214,7 +215,7 @@
             peaks[i] = jnp.max(s, axis=0, keepdims=True) * factor2
 
         def soften(i):
-            c, p = todo[i]
+            c, p, slot = todo[i]
             peak = peaks.pop(i)
             shrink = None
             if not diagonal:
@@ -228,7 +229,7 @@
             ready[i] = (w.astype(BF), shrink)
 
         def gather(i):
-            c, p = todo[i]
+            c, p, slot = todo[i]
             w, shrink = ready.pop(i)
             o = dot(vt[slot, p * LANES : (p + 1) * LANES, : keys(c)], w)
             o = jnp.concatenate([o[:VDIM, :chunk], o[VDIM:, chunk:]], axis=1)
@@ -252,14 +253,21 @@
         column = jnp.logical_and(j >= 0, turn_of == 0)
         return (z - level) * nx + across_x, column
 
-    def pump(k, r):
+    def pump(q):
+        k, r = q // count + 1, q % count
+
         @pl.when(k <= z)
         def _():
             src = sp - k * nx
             arrival(src, r).wait_recv()
-            share(src, r).start()
+
+            @pl.when(z < nz - 1)
+            def _():
+                up_copy(k, r).start()
+
             for step in range(1, nx):
                 relay(k, r, step).start()
+            share(src, r).start()
 
     def fetch(i):
         src, column = place_of(i)
@@ -279,10 +287,9 @@
         with jax.named_scope("pump"):
             @pl.when(i > 0)
             def _():
-                for r in range(count - 1):
-                    pump(i + 2, r)
-
-            pump(i + 2, count - 1)
+                pump(3 + 2 * i)
+                pump(4 + 2 * i)
+
         with jax.named_scope("fetch"):
             fetch(i + 1)
 
@@ -307,6 +314,8 @@
         wide = jnp.concatenate([buf[s, here] for s in range(n)], axis=1).astype(F32)
         factor = lax.rsqrt(jnp.sum(wide * wide, axis=1, keepdims=True) / (n * width) + EPSILON)
         scaled = (wide * pre[...]).astype(BF)
+        scale_of[here] = scaled
+        factors[here] = jnp.broadcast_to(factor, (chunk, LANES))
         flat = jnp.broadcast_to(factor, (chunk, LANES)).T[:1]
         cosine, sine = angle[: ROPE // 2, here], angle[ROPE // 2 :, here]
 
@@ -323,10 +332,10 @@
         kvs[sp, r, chunk:] = jnp.concatenate(
             [key[g * TURN : (g + 1) * TURN] for g in range(ROPE // TURN)], axis=1
         ).astype(BF)
-        for k in range(1, nz):
-            @pl.when(z + k < nz)
-            def _(k=k):
-                column_copy(r, k).start()
+        @pl.when(z < nz - 1)
+        def _():
+            up_copy(0, r).start()
+
         for step in range(1, nx):
             @pl.when(x + step < nx)
             def _(step=step):
@@ -342,9 +351,7 @@
             if r + 1 < count:
                 pass_on(r + 1)
             else:
-                for k in range(1, min(nz, 3)):
-                    for early in range(count - 2):
-                        pump(k, early)
+                pump(0)
         query = dot_nt(vut[...], q.astype(BF))
         for h in range(heads):
             p, low_half = h // 2, h % 2
@@ -358,10 +365,9 @@
                 query[base + NOPE : middle], query[middle : base + NOPE + ROPE]
             ).astype(BF)
 
-        if r == 0:
-            with jax.named_scope("wload6"):
-                for load in loads[6:9]:
-                    load.wait()
+    def branch(r):
+        here = part(r)
+        scaled, factor = scale_of[here], factors[here, :1]
         inner = (dot(scaled, vi[...]) * factor).astype(BF).astype(F32)
         source = (dot(scaled, vs[...]) * factor).astype(BF).astype(F32)
         driven = (inner * source).astype(BF)
@@ -373,25 +379,37 @@
             def _():
                 halo_copy().start()
         outer[here] = (dot(scaled, vo[...]) * factor).astype(BF)
-        if r == count - 1:
-            with jax.named_scope("prefetch"):
-                for k in range(1, min(nz, 3)):
-                    pump(k, count - 2)
-                fetch(0)
-                pump(1, count - 1)
+
+    def diagonal(r):
         with jax.named_scope(f"diag{r}"):
             raise_keys(sp, 0, [r])
-            units([(r, p) for p in range(pairs)], 0, True)
+            units([(r, p, 0) for p in range(pairs)], True)
 
     for r in range(count):
         project(r)
+    with jax.named_scope("wload6"):
+        for load in loads[6:9]:
+            load.wait()
+    with jax.named_scope("pump1"):
+        pump(1)
+    for r in range(count - 1, -1, -1):
+        with jax.named_scope("branch"):
+            branch(r)
+    with jax.named_scope("prefetch"):
+        fetch(0)
+        pump(2)
+        pump(3)
+    for r in range(count):
+        diagonal(r)
+    with jax.named_scope("pump4"):
+        pump(4)
 
     wave = jnp.minimum(items, WAVE)
 
     def whole(i, carry):
         take(i, 0)
         with jax.named_scope("units"):
-          units([(c, p) for c in range(count) for p in range(pairs)], 0, False)
+          units([(c, p, 0) for c in range(count) for p in range(pairs)], False)
         return carry
 
     lax.fori_loop(0, items - wave, whole, 0)
@@ -450,14 +468,19 @@
             across(c, step).start()
 
     for c in range(count):
-        def last(w, carry, c=c):
+        @pl.when(items >= WAVE)
+        def _(c=c):
             with jax.named_scope("lastunits"):
-                units([(c, p) for p in range(pairs)], w, False)
-            return carry
-
-        lax.fori_loop(0, wave, last, 0)
-        if c > 0:
-            send_on(c - 1)
+                units([(c, p, w) for w in range(WAVE) for p in range(pairs)], False)
+
+        @pl.when(items < WAVE)
+        def _(c=c):
+            def last(w, carry):
+                units([(c, p, w) for p in range(pairs)], False)
+                return carry
+
+            lax.fori_loop(0, items, last, 0)
+
         for p in range(pairs):
             value = acc[c, p] / low[c, p]
             both = jnp.concatenate([value[:, :chunk], value[:, chunk:]], axis=0)
@@ -478,8 +501,46 @@
         peer[part(c)] = product(c, partner)
         home(c).start()
         total[part(c)] = product(c, tp).astype(F32)
-        if c == count - 1:
-            send_on(c)
+        send_on(c)
+    for r in range(count):
+        own_copy(r).wait_send()
+        for step in range(1, ny):
+            y_copy(r, step).wait_send()
+            forward(r, lax.rem(y + step, ny)).wait_send()
+        for step in range(1, nx):
+            @pl.when(x + step < nx)
+            def _(step=step, r=r):
+                own_side(r, step).wait_send()
+
+    @pl.when(sp < nsp - 1)
+    def _():
+        halo_copy().wait_send()
+
+    def sent(i, carry):
+        src, _ = place_of(i)
+        for r in range(count):
+            share(src, r).wait_send()
+        return carry
+
+    lax.fori_loop(0, items, sent, 0)
+
+    def relayed(k, carry):
+        for r in range(count):
+            for step in range(1, nx):
+                relay(k, r, step).wait_send()
+        return carry
+
+    lax.fori_loop(1, z + 1, relayed, 0)
+
+    @pl.when(z < nz - 1)
+    def _():
+        def raised(k, carry):
+            for r in range(count):
+                up_copy(k, r).wait_send()
+            return carry
+
+        lax.fori_loop(0, z + 1, raised, 0)
+
     for r in range(count):
         with jax.named_scope("homewait"):
             home(r).wait_recv()
@@ -499,51 +560,19 @@
             with jax.named_scope("sqwait"):
                 squares(r, step).wait_recv()
             whole_sum = whole_sum + sqin[step, r]
-        scale = lax.rsqrt(whole_sum / (n * width) + EPSILON)
-        column = jnp.broadcast_to(scale[:1], (LANES, chunk)).T[:, :1]
-        out[part(r)] = (total[part(r)] * column * gain[...]).astype(BF)
-
-    with jax.named_scope("endsends"):
-        own_copy(0).wait_send()
-    for r in range(count):
-        if r > 0:
-            own_copy(r).wait_send()
+        with jax.named_scope("outs"):
+          scale = lax.rsqrt(whole_sum / (n * width) + EPSILON)
+          column = jnp.broadcast_to(scale[:1], (LANES, chunk)).T[:, :1]
+          out[part(r)] = (total[part(r)] * column * gain[...]).astype(BF)
+
+    with jax.named_scope("endsend"):
+     for r in range(count):
         home(r).wait_send()
         for step in range(1, ny):
-            y_copy(r, step).wait_send()
-            forward(r, lax.rem(y + step, ny)).wait_send()
             to_partner(r, step).wait_send()
             across(r, step).wait_send()
         for step in range(1, n):
             squares(r, step).wait_send()
-        for k in range(1, nz):
-            @pl.when(z + k < nz)
-            def _(k=k, r=r):
-                column_copy(r, k).wait_send()
-        for step in range(1, nx):
-            @pl.when(x + step < nx)
-            def _(step=step, r=r):
-                own_side(r, step).wait_send()
-
-    @pl.when(sp < nsp - 1)
-    def _():
-        halo_copy().wait_send()
-
-    def sent(i, carry):
-        src, _ = place_of(i)
-        for r in range(count):
-            share(src, r).wait_send()
-        return carry
-
-    lax.fori_loop(0, items, sent, 0)
-
-    def relayed(k, carry):
-        for r in range(count):
-            for step in range(1, nx):
-                relay(k, r, step).wait_send()
-        return carry
-
-    lax.fori_loop(1, z + 1, relayed, 0)
 
 
 DMA = pltpu.SemaphoreType.DMA
@@ -600,6 +629,7 @@
             v((AHEAD + 2, rows, 2 * chunk), F32),
             v((count, pairs, VDIM, 2 * chunk), F32),
             v((count, pairs, 1, 2 * chunk), F32), v((count, pairs, 1, 2 * chunk), F32),
+            v((rows, ntp * width), BF), v((rows, LANES), F32),
             v((rows, channels), BF), v((8 + rows, channels), F32),
             v((HALO, channels), BF), v((HALO, channels), BF),
             v((rows, heads * VDIM + channels), BF),
@@ -610,7 +640,7 @@
             v((count, 8, chunk), F32), v((ntp, count, 8, chunk), F32),
             DMA((count,)), DMA((11,)), DMA((count,)), DMA((count,)),
             DMA((count, ny)), DMA((count, ny)), DMA((count, ny)), DMA((count, ny)),
-            DMA((count, nz)), DMA((count, nx)), DMA((nz, count, nx)),
+            DMA((nz, count)), DMA((count, nx)), DMA((nz, count, nx)),
             DMA((nsp, count)), DMA((nsp, count)), DMA((nsp, count)), DMA((1,)), DMA((1,)),
             DMA((count, ny)), DMA((count, ny)), DMA((count, ny)), DMA((count, ny)),
             DMA((count,)), DMA((count,)), DMA((count, ntp)), DMA((count, ntp)),

time: 64.2 us -> 57.3 us (0.89)
  Pallas kernels: 62 us -> 55.1 us
    pallas_call x1, Pallas kernels: 62 us -> 55.1 us  [body(): pl.pallas_call(functools.partial(layer_kernel, nz, nx, ntp, chunk, heads)...]
where the time goes in v3:
time: 57.3 us; the launch traced here: 57.1 us
  Pallas kernels  55.1 us (96%)
  local copies, waits for them, and re-layouts  1.35 us (2%)
  between operations  0.65 us (1%)
    pallas_call x1, Pallas kernels, body(): pl.pallas_call(functools.partial(layer_kernel, nz, nx, ntp, chunk, heads)...  55.1 us
    unnamed x2, local copies, waits for them, and re-layouts  1.35 us

profile of v3, /device:TPU:27, one launch (start us, length us, event | category | flops | bytes accessed | tf_op | source)
XLA Modules:
  0.0 57.1 jit_solution(7628975531666347689)
XLA Ops:
  0.6 55.1 %layer.1 = (bf16[384,512]{1,0:T(8,128)(2,1)S(1)}, f32[8,384]{1,0:T(8,128)S(1)}) custom-call(bf16[384,512]{1,0:T(8,128)(2,1)} %tok.1, f32[1,2048]{1,0:T(1,128)} %bitcast.6, f32[6,128]{1,0:T(8,128)} %bitcast.7, f32[1,512]{1,0:T(1,128)} %bitcast.8, f32[1,512]{1,0:T(1,128)} %bitcast.9, bf16[3,256]{1,0:T(4,128)(2,1)} %taps.1, f32[32,3072]{1,0:T(8,128)} %constant.2.clone.table, ...), custom_call_target="tpu_custom_call" | custom-call | tf_op jit(solution)/shard_map/layer/pallas_call | solution.py:614
  55.7 0.7 %copy.21 = bf16[384,512]{1,0:T(8,128)(2,1)} copy(bf16[384,512]{1,0:T(8,128)(2,1)S(1)} %get-tuple-element.2) | data formatting | bytes 786432
  56.5 0.6 %copy.22 = f32[8,384]{1,0:T(8,128)} copy(f32[8,384]{1,0:T(8,128)S(1)} %get-tuple-element.3) | data formatting | bytes 24576

commit v4 on v3

--- a/solution.py
+++ b/solution.py
@@ -102,54 +102,68 @@
     def y_copy(r, step):
         to = lax.rem(y + step, ny) * 2 + core
         here = buf.at[tp, part(r)]
-        return remote(here, here, y_s.at[r, step], y_r.at[r, y], tp=to)
-
-    def y_arrival(r, other):
-        here = buf.at[other * 2 + core, part(r)]
-        return remote(here, here, y_s.at[r, 0], y_r.at[r, other], tp=partner)
+        return remote(here, here, y_s.at[step - 1], y_r.at[r, step - 1], tp=to)
+
+    def y_other(step):
+        return lax.rem(y + ny - step, ny)
+
+    def y_arrival(r, step):
+        here = buf.at[y_other(step) * 2 + core, part(r)]
+        return remote(here, here, y_s.at[step - 1], y_r.at[r, step - 1], tp=partner)
 
     def own_copy(r):
         here = buf.at[tp, part(r)]
-        return remote(here, here, own_s.at[r], own_r.at[r], tp=partner)
+        return remote(here, here, own_s.at[0], own_r.at[r], tp=partner)
 
     def own_arrival(r):
         here = buf.at[partner, part(r)]
-        return remote(here, here, own_s.at[r], own_r.at[r], tp=partner)
-
-    def forward(r, other):
-        here = buf.at[other * 2 + core, part(r)]
-        return remote(here, here, f_s.at[r, other], f_r.at[r, other], tp=partner)
-
-    def forward_arrival(r, other):
-        here = buf.at[other * 2 + 1 - core, part(r)]
-        return remote(here, here, f_s.at[r, other], f_r.at[r, other], tp=partner)
+        return remote(here, here, own_s.at[0], own_r.at[r], tp=partner)
+
+    def forward(r, step):
+        here = buf.at[y_other(step) * 2 + core, part(r)]
+        return remote(here, here, f_s.at[step - 1], f_r.at[r, step - 1], tp=partner)
+
+    def forward_arrival(r, step):
+        here = buf.at[y_other(step) * 2 + 1 - core, part(r)]
+        return remote(here, here, f_s.at[step - 1], f_r.at[r, step - 1], tp=partner)
+
+    def tokens_sent():
+        here = buf.at[tp]
+        remote(here, here, own_s.at[0], own_r.at[0], tp=partner).wait_send()
+        for step in range(1, ny):
+            remote(here, here, y_s.at[step - 1], own_r.at[0], tp=partner).wait_send()
+            remote(here, here, f_s.at[step - 1], own_r.at[0], tp=partner).wait_send()
 
     def piece(src, r):
         return kvs.at[src, r, :, side]
 
     def up_copy(k, r):
         src = sp - k * nx
-        return remote(piece(src, r), piece(src, r), z_s.at[k, r], i_r.at[src, r], sp=sp + nx)
+        return remote(piece(src, r), piece(src, r), z_s.at[k], i_r.at[src, r], sp=sp + nx)
 
     def own_side(r, step):
         to = z * nx + lax.rem(x + step, nx)
-        return remote(piece(sp, r), piece(sp, r), o_s.at[r, step], i_r.at[sp, r], sp=to)
+        return remote(piece(sp, r), piece(sp, r), o_s.at[step - 1], i_r.at[sp, r], sp=to)
 
     def relay(k, r, step):
         src = sp - k * nx
         to = z * nx + lax.rem(x + step, nx)
-        return remote(piece(src, r), piece(src, r), x_s.at[k, r, step], i_r.at[src, r], sp=to)
+        return remote(piece(src, r), piece(src, r), x_s.at[k - 1, step - 1], i_r.at[src, r], sp=to)
 
     def arrival(src, r):
-        return remote(piece(src, r), piece(src, r), z_s.at[0, r], i_r.at[src, r], tp=partner)
+        return remote(piece(src, r), piece(src, r), z_s.at[0], i_r.at[src, r], tp=partner)
 
     def share(src, r):
-        return remote(piece(src, r), piece(src, r), d_s.at[src, r], d_r.at[src, r], tp=partner)
-
-    def share_arrival(src, r):
+        return remote(piece(src, r), piece(src, r), d_s.at[src], d_r.at[src], tp=partner)
+
+    def share_arrival(src):
         other = pl.ds(pl.multiple_of((1 - core) * (rank // 2), LANES), rank // 2)
-        here = kvs.at[src, r, :, other]
-        return remote(here, here, d_s.at[src, r], d_r.at[src, r], tp=partner)
+        here = kvs.at[src, :, :, other]
+        return remote(here, here, d_s.at[src], d_r.at[src], tp=partner)
+
+    def block_sent(sem):
+        here = kvs.at[sp, :, :, side]
+        remote(here, here, sem, d_r.at[0], tp=partner).wait_send()
 
     def halo_copy():
         return remote(tail, halo, h_s.at[0], h_r.at[0], sp=sp + 1)
@@ -177,12 +191,18 @@
         upvt[h * VDIM : (h + 1) * VDIM] = turned[h * LANES + NOPE : (h + 1) * LANES]
 
     def raise_keys(src, slot, span):
-        count_here = len(span)
-        lat = jnp.concatenate([kvs[src, r, : chunk] for r in span], axis=0)
-        here = pl.ds(span[0] * chunk, count_here * chunk)
-        kn[slot, here] = dot(lat, upk[...]).astype(BF)
-        vt[slot, :, here] = dot_nt(upvt[...], lat).astype(BF)
-        for r in span:
+        here = pl.ds(span[0] * chunk, len(span) * chunk)
+
+        def latent():
+            return jnp.concatenate([kvs[src, r, :chunk] for r in span], axis=0)
+
+        def keys(start, stop):
+            kn[slot, here, start:stop] = dot(latent(), upk[:, start:stop]).astype(BF)
+
+        def values():
+            vt[slot, :, here] = dot_nt(upvt[...], latent()).astype(BF)
+
+        def turns(r):
             packed = kvs[src, r, chunk:].astype(F32)
             tall = jnp.concatenate(
                 [packed[:, g * LANES : (g + 1) * LANES] for g in range(ROPE // TURN)]
@@ -191,7 +211,16 @@
             )
             turn[slot, part(r)] = tall.T.astype(BF)
 
-    def units(todo, diagonal):
+        wide = heads * NOPE
+        cut = min(wide, 2 * LANES)
+        parts = [functools.partial(keys, s, s + cut) for s in range(0, wide, cut)]
+        return parts + [values] + [functools.partial(turns, r) for r in span]
+
+    def do(parts):
+        for one in parts:
+            one()
+
+    def units(todo, diagonal, parts=()):
         peaks, ready = {}, {}
         size = len(todo)
 
@@ -235,22 +264,33 @@
             o = jnp.concatenate([o[:VDIM, :chunk], o[VDIM:, chunk:]], axis=1)
             acc[c, p] = o if diagonal else acc[c, p] * shrink + o
 
+        parts = list(parts)
         for t in range(size + AHEAD + 1):
             if t < size:
                 score(t)
+            if parts:
+                parts.pop(0)()
             if 0 <= t - AHEAD < size:
                 soften(t - AHEAD)
             if 0 <= t - AHEAD - 1 < size:
                 gather(t - AHEAD - 1)
+        do(parts)
 
     items = z * nx + x
 
     def place_of(i):
-        j = i - x
-        turn_of = lax.rem(j + nx, nx)
-        across_x = jnp.where(j < 0, i, lax.rem(x + turn_of, nx))
-        level = jnp.where(j < 0, 0, j // nx + 1)
-        column = jnp.logical_and(j >= 0, turn_of == 0)
+        j = i - x - 1
+        block, spot = (j + nx) // nx - 1, lax.rem(j + nx, nx)
+        late = block >= z - 1
+        column = jnp.where(late, False, spot == 0)
+        step = jnp.where(late, spot + 1, spot)
+        level = jnp.where(late, z, jnp.where(spot == 0, block + 2, block + 1))
+        column = jnp.logical_or(j == -1, column)
+        step = jnp.where(j == -1, 0, step)
+        level = jnp.where(j == -1, 1, level)
+        level = jnp.where(j < -1, 0, level)
+        column = jnp.logical_and(j >= -1, column)
+        across_x = jnp.where(j < -1, i, lax.rem(x + step, nx))
         return (z - level) * nx + across_x, column
 
     def pump(q):
@@ -278,26 +318,22 @@
                 arrival(src, r).wait_recv()
                 share(src, r).start()
 
-    def take(i, slot):
+    def shared(i):
         src, _ = place_of(i)
         with jax.named_scope("sharewait"):
-            for r in range(count):
-                share_arrival(src, r).wait_recv()
-        raise_keys(src, slot, list(range(count)))
+            share_arrival(src).wait_recv()
+
+    def prepare(i):
         with jax.named_scope("pump"):
-            @pl.when(i > 0)
-            def _():
-                pump(3 + 2 * i)
-                pump(4 + 2 * i)
-
+            pump(5 + 2 * i)
+            pump(6 + 2 * i)
         with jax.named_scope("fetch"):
-            fetch(i + 1)
+            fetch(i + 2)
 
     def pass_on(r):
         for step in range(1, ny):
-            other = lax.rem(y + ny - step, ny)
-            y_arrival(r, other).wait_recv()
-            forward(r, other).start()
+            y_arrival(r, step).wait_recv()
+            forward(r, step).start()
 
     def project(r):
         with jax.named_scope(f"tokwait{r}"):
@@ -305,7 +341,7 @@
                 pass_on(r)
             own_arrival(r).wait_recv()
             for step in range(1, ny):
-                forward_arrival(r, lax.rem(y + ny - step, ny)).wait_recv()
+                forward_arrival(r, step).wait_recv()
         if r == 0:
             with jax.named_scope("wload2"):
                 for load in loads[2:5]:
@@ -380,11 +416,6 @@
                 halo_copy().start()
         outer[here] = (dot(scaled, vo[...]) * factor).astype(BF)
 
-    def diagonal(r):
-        with jax.named_scope(f"diag{r}"):
-            raise_keys(sp, 0, [r])
-            units([(r, p, 0) for p in range(pairs)], True)
-
     for r in range(count):
         project(r)
     with jax.named_scope("wload6"):
@@ -397,28 +428,57 @@
             branch(r)
     with jax.named_scope("prefetch"):
         fetch(0)
+        fetch(1)
         pump(2)
         pump(3)
-    for r in range(count):
-        diagonal(r)
+    with jax.named_scope("diag"):
+        do(raise_keys(sp, 0, list(range(count))))
+        units([(r, p, 0) for r in range(count) for p in range(pairs)], True)
     with jax.named_scope("pump4"):
         pump(4)
 
-    wave = jnp.minimum(items, WAVE)
-
-    def whole(i, carry):
-        take(i, 0)
-        with jax.named_scope("units"):
-          units([(c, p, 0) for c in range(count) for p in range(pairs)], False)
-        return carry
-
-    lax.fori_loop(0, items - wave, whole, 0)
-
-    def ready(w, carry):
-        take(items - wave + w, w)
-        return carry
-
-    lax.fori_loop(0, wave, ready, 0)
+    everything = list(range(count))
+    many = items >= WAVE
+
+    @pl.when(many)
+    def _():
+        shared(0)
+        with jax.named_scope("raise0"):
+            do(raise_keys(place_of(0)[0], 0, everything))
+
+        def whole(i, carry):
+            prepare(i)
+            shared(i + 1)
+            with jax.named_scope("units"):
+                units(
+                    [(c, p, 0) for c in everything for p in range(pairs)], False,
+                    raise_keys(place_of(i + 1)[0], 1, everything),
+                )
+                for old in (kn, vt, turn):
+                    old[0] = old[1]
+            return carry
+
+        lax.fori_loop(0, items - WAVE, whole, 0)
+        for w in range(WAVE - 1):
+            prepare(items - WAVE + w)
+            shared(items - WAVE + w + 1)
+            with jax.named_scope("waveunits"):
+                units(
+                    [(0, p, w) for p in range(pairs)], False,
+                    raise_keys(place_of(items - WAVE + w + 1)[0], w + 1, everything),
+                )
+        with jax.named_scope("waveunits"):
+            units([(0, p, WAVE - 1) for p in range(pairs)], False)
+
+    @pl.when(jnp.logical_not(many))
+    def _():
+        def ready(w, carry):
+            prepare(w)
+            shared(w)
+            do(raise_keys(place_of(w)[0], w, everything))
+            return carry
+
+        lax.fori_loop(0, items, ready, 0)
 
     @pl.when(sp == 0)
     def _():
@@ -438,21 +498,21 @@
 
     def to_partner(r, step):
         return remote(
-            away.at[step, part(r)], pin.at[step, part(r)], a_s.at[r, step], a_r.at[r, step], tp=partner
+            away.at[step, part(r)], pin.at[step, part(r)], a_s.at[step - 1], a_r.at[r, step - 1], tp=partner
         )
 
     def across(r, step):
         to = lax.rem(y + step, ny) * 2 + core
         return remote(
-            ysend.at[step, part(r)], yin.at[step, part(r)], b_s.at[r, step], b_r.at[r, step], tp=to
+            ysend.at[step, part(r)], yin.at[step, part(r)], b_s.at[step - 1], b_r.at[r, step - 1], tp=to
         )
 
     def home(r):
-        return remote(peer.at[part(r)], pown.at[part(r)], p_s.at[r], p_r.at[r], tp=partner)
+        return remote(peer.at[part(r)], pown.at[part(r)], p_s.at[0], p_r.at[r], tp=partner)
 
     def squares(r, step):
         return remote(
-            sq.at[r], sqin.at[step, r], q_s.at[r, step], q_r.at[r, step], tp=lax.rem(tp + step, n)
+            sq.at[r], sqin.at[step, r], q_s.at[step - 1], q_r.at[r, step - 1], tp=lax.rem(tp + step, n)
         )
 
     for load in loads[9:]:
@@ -468,12 +528,13 @@
             across(c, step).start()
 
     for c in range(count):
-        @pl.when(items >= WAVE)
-        def _(c=c):
-            with jax.named_scope("lastunits"):
-                units([(c, p, w) for w in range(WAVE) for p in range(pairs)], False)
-
-        @pl.when(items < WAVE)
+        if c > 0:
+            @pl.when(many)
+            def _(c=c):
+                with jax.named_scope("lastunits"):
+                    units([(c, p, w) for w in range(WAVE) for p in range(pairs)], False)
+
+        @pl.when(jnp.logical_not(many))
         def _(c=c):
             def last(w, carry):
                 units([(c, p, w) for p in range(pairs)], False)
@@ -502,32 +563,25 @@
         home(c).start()
         total[part(c)] = product(c, tp).astype(F32)
         send_on(c)
-    for r in range(count):
-        own_copy(r).wait_send()
-        for step in range(1, ny):
-            y_copy(r, step).wait_send()
-            forward(r, lax.rem(y + step, ny)).wait_send()
-        for step in range(1, nx):
-            @pl.when(x + step < nx)
-            def _(step=step, r=r):
-                own_side(r, step).wait_send()
+    tokens_sent()
+    for step in range(1, nx):
+        @pl.when(x + step < nx)
+        def _(step=step):
+            block_sent(o_s.at[step - 1])
 
     @pl.when(sp < nsp - 1)
     def _():
         halo_copy().wait_send()
 
     def sent(i, carry):
-        src, _ = place_of(i)
-        for r in range(count):
-            share(src, r).wait_send()
+        block_sent(d_s.at[place_of(i)[0]])
         return carry
 
     lax.fori_loop(0, items, sent, 0)
 
     def relayed(k, carry):
-        for r in range(count):
-            for step in range(1, nx):
-                relay(k, r, step).wait_send()
+        for step in range(1, nx):
+            block_sent(x_s.at[k - 1, step - 1])
         return carry
 
     lax.fori_loop(1, z + 1, relayed, 0)
@@ -535,8 +589,7 @@
     @pl.when(z < nz - 1)
     def _():
         def raised(k, carry):
-            for r in range(count):
-                up_copy(k, r).wait_send()
+            block_sent(z_s.at[k])
             return carry
 
         lax.fori_loop(0, z + 1, raised, 0)
@@ -565,14 +618,12 @@
           column = jnp.broadcast_to(scale[:1], (LANES, chunk)).T[:, :1]
           out[part(r)] = (total[part(r)] * column * gain[...]).astype(BF)
 
-    with jax.named_scope("endsend"):
-     for r in range(count):
-        home(r).wait_send()
-        for step in range(1, ny):
-            to_partner(r, step).wait_send()
-            across(r, step).wait_send()
-        for step in range(1, n):
-            squares(r, step).wait_send()
+    remote(peer, pown, p_s.at[0], p_r.at[0], tp=partner).wait_send()
+    for step in range(1, ny):
+        remote(peer, pown, a_s.at[step - 1], p_r.at[0], tp=partner).wait_send()
+        remote(peer, pown, b_s.at[step - 1], p_r.at[0], tp=partner).wait_send()
+    for step in range(1, n):
+        remote(sq, sqin.at[step], q_s.at[step - 1], p_r.at[0], tp=partner).wait_send()
 
 
 DMA = pltpu.SemaphoreType.DMA
@@ -638,12 +689,12 @@
         + [
             v((rows, width), BF), v((rows, width), BF), v((rows, width), F32),
             v((count, 8, chunk), F32), v((ntp, count, 8, chunk), F32),
-            DMA((count,)), DMA((11,)), DMA((count,)), DMA((count,)),
-            DMA((count, ny)), DMA((count, ny)), DMA((count, ny)), DMA((count, ny)),
-            DMA((nz, count)), DMA((count, nx)), DMA((nz, count, nx)),
-            DMA((nsp, count)), DMA((nsp, count)), DMA((nsp, count)), DMA((1,)), DMA((1,)),
-            DMA((count, ny)), DMA((count, ny)), DMA((count, ny)), DMA((count, ny)),
-            DMA((count,)), DMA((count,)), DMA((count, ntp)), DMA((count, ntp)),
+            DMA((count,)), DMA((11,)), DMA((1,)), DMA((count,)),
+            DMA((ny - 1,)), DMA((count, ny - 1)), DMA((ny - 1,)), DMA((count, ny - 1)),
+            DMA((nz,)), DMA((nx - 1,)), DMA((nz - 1, nx - 1)),
+            DMA((nsp, count)), DMA((nsp,)), DMA((nsp,)), DMA((1,)), DMA((1,)),
+            DMA((ny - 1,)), DMA((count, ny - 1)), DMA((ny - 1,)), DMA((count, ny - 1)),
+            DMA((1,)), DMA((count,)), DMA((ntp - 1,)), DMA((count, ntp - 1)),
         ],
         compiler_params=pltpu.CompilerParams(
             collective_id=0, has_side_effects=True, vmem_limit_bytes=60 * 1024 * 1024

time: 57.3 us -> 56.2 us (0.981)
  Pallas kernels: 55.1 us -> 53.9 us
    pallas_call x1, Pallas kernels: 55.1 us -> 53.9 us  [body(): pl.pallas_call(functools.partial(layer_kernel, nz, nx, ntp, chunk, heads)...]
where the time goes in v4:
time: 56.2 us; the launch traced here: 55.9 us
  Pallas kernels  53.9 us (96%)
  local copies, waits for them, and re-layouts  1.35 us (2%)
  between operations  0.65 us (1%)
    pallas_call x1, Pallas kernels, body(): pl.pallas_call(functools.partial(layer_kernel, nz, nx, ntp, chunk, heads)...  53.9 us
    unnamed x2, local copies, waits for them, and re-layouts  1.35 us

profile of v4, /device:TPU:27, one launch (start us, length us, event | category | flops | bytes accessed | tf_op | source)
XLA Modules:
  0.0 55.9 jit_solution(7087673998531390937)
XLA Ops:
  0.6 53.9 %layer.1 = (bf16[384,512]{1,0:T(8,128)(2,1)S(1)}, f32[8,384]{1,0:T(8,128)S(1)}) custom-call(bf16[384,512]{1,0:T(8,128)(2,1)} %tok.1, f32[1,2048]{1,0:T(1,128)} %bitcast.6, f32[6,128]{1,0:T(8,128)} %bitcast.7, f32[1,512]{1,0:T(1,128)} %bitcast.8, f32[1,512]{1,0:T(1,128)} %bitcast.9, bf16[3,256]{1,0:T(4,128)(2,1)} %taps.1, f32[32,3072]{1,0:T(8,128)} %constant.2.clone.table, ...), custom_call_target="tpu_custom_call" | custom-call | tf_op jit(solution)/shard_map/layer/pallas_call | solution.py:665
  54.6 0.7 %copy.21 = bf16[384,512]{1,0:T(8,128)(2,1)} copy(bf16[384,512]{1,0:T(8,128)(2,1)S(1)} %get-tuple-element.2) | data formatting | bytes 786432
  55.3 0.6 %copy.22 = f32[8,384]{1,0:T(8,128)} copy(f32[8,384]{1,0:T(8,128)S(1)} %get-tuple-element.3) | data formatting | bytes 24576

commit v5 on v4

--- a/solution.py
+++ b/solution.py
@@ -43,11 +43,11 @@
 
 def layer_kernel(
     nz, nx, n, chunk, heads,
-    tok, pre, qg, kg, gain, taps, table, wo, wi, ws, wq, wk, wr, wu, wkv, wa, wc,
+    tok, pre_in, qg_in, kg_in, gain_in, taps_in, table, wo, wi, ws, wq, wk, wr, wu, wkv, wa, wc,
     out, logs,
-    buf, vo, vi, vs, vq, vk, vr, vu, vkv, va, vc, angle,
+    pre, qg, kg, gain, taps, buf, vo, vi, vs, vq, vk, vr, vu, vkv, va, vc, angle,
     vut, upk, upvt, qt, kvs, kn, turn, vt, sbuf, acc, top, low,
-    scale_of, factors, outer, ext, tail, halo, att,
+    near, near_square, near_k, near_r, near_q, near_c, far, factors, outer, ext, tail, halo, att,
     away, mine, pin, ysend, yin, peer, pown, total, sq, sqin,
     t_s, w_s, own_s, own_r, y_s, y_r, f_s, f_r,
     z_s, o_s, x_s, i_r, d_s, d_r, h_s, h_r,
@@ -74,8 +74,9 @@
     ]
     place = pl.ds(pl.multiple_of(sp * rows, LANES), rows)
     pairs_of = (
-        (wu, vu), (wkv, vkv), (table.at[:, place], angle), (wk, vk), (wr, vr), (wq, vq),
-        (wi, vi), (ws, vs), (wo, vo), (wa, va), (wc, vc),
+        (wk, vk), (wr, vr), (wq, vq), (wi, vi), (ws, vs), (wo, vo), (wu, vu), (wkv, vkv),
+        (table.at[:, place], angle), (qg_in, qg), (kg_in, kg), (pre_in, pre),
+        (wa, va), (wc, vc), (gain_in, gain), (taps_in, taps),
     )
     loads = [pltpu.make_async_copy(a, b, w_s.at[i]) for i, (a, b) in enumerate(pairs_of)]
     for token in tokens:
@@ -88,16 +89,23 @@
 
     for step in range(1, n):
         greet(tp=lax.rem(tp + step, n))
-    greet(sp=lax.rem(z + 1, nz) * nx + x)
-    greet(sp=lax.rem(z + nz - 1, nz) * nx + x)
+    for live, there in (
+        (z > 0, sp - nx), (z < nz - 1, sp + nx), (sp > 0, sp - 1), (sp < nsp - 1, sp + 1)
+    ):
+        @pl.when(live)
+        def _(there=there):
+            greet(sp=there)
+
     for step in range(1, nx):
         greet(sp=z * nx + lax.rem(x + step, nx))
-    greet(sp=lax.rem(sp + 1, nsp))
-    greet(sp=lax.rem(sp + nsp - 1, nsp))
-    for load in loads:
+    heard = sum(
+        jnp.where(live, 1, 0) for live in (z > 0, z < nz - 1, sp > 0, sp < nsp - 1)
+    )
+    loads[11].start()
+    for load in loads[:11] + loads[12:]:
         load.start()
     with jax.named_scope("barrier"):
-        pl.semaphore_wait(barrier, n - 1 + 2 + nx - 1 + 2)
+        pl.semaphore_wait(barrier, n - 1 + nx - 1 + heard)
 
     def y_copy(r, step):
         to = lax.rem(y + step, ny) * 2 + core
@@ -175,20 +183,47 @@
                 y_copy(r, step).start()
             own_copy(r).start()
 
+    def lanes_of(other):
+        return pl.ds(pl.multiple_of(other * 2 * width, LANES), 2 * width)
+
+    def pick(other, here):
+        return jnp.concatenate([buf[other * 2, here], buf[other * 2 + 1, here]], axis=1).astype(F32)
+
+    def load_wait(start, stop):
+        with jax.named_scope(f"wload{start}"):
+            for load in loads[start:stop]:
+                load.wait()
+
+    qt[...] = jnp.zeros_like(qt)
+    with jax.named_scope("ownwait"):
+        for r in range(count):
+            own_arrival(r).wait_recv()
+    mine_here = lanes_of(y)
+    load_wait(11, 12)
+    wide = pick(y, pl.ds(0, rows))
+    near_square[...] = jnp.broadcast_to(jnp.sum(wide * wide, axis=1, keepdims=True), (rows, LANES))
+    near[...] = (wide * pre[:, mine_here]).astype(BF)
+    load_wait(0, 2)
+    near_k[...] = dot(near[...], vk[mine_here])
+    near_r[...] = dot_nt(vr[:, mine_here], near[...])
+    load_wait(2, 3)
+    near_q[...] = dot(near[...], vq[mine_here])
+    load_wait(3, 6)
+    channels = vi.shape[1]
+    for index, w in enumerate((vi, vs, vo)):
+        near_c[:, index * channels : (index + 1) * channels] = dot(near[...], w[mine_here])
+
+    load_wait(6, 11)
     with jax.named_scope("wturn"):
-        qt[...] = jnp.zeros_like(qt)
-        loads[0].wait()
         vut[...] = vu[...].T
-    with jax.named_scope("wload1"):
-        loads[1].wait()
-    for p in range(pairs):
-        first, second = 2 * p * LANES, (2 * p + 1) * LANES
-        upk[:, p * LANES : (p + 1) * LANES] = jnp.concatenate(
-            [vkv[:, first : first + NOPE], vkv[:, second : second + NOPE]], axis=1
-        )
-    turned = vkv[...].T
-    for h in range(heads):
-        upvt[h * VDIM : (h + 1) * VDIM] = turned[h * LANES + NOPE : (h + 1) * LANES]
+        for p in range(pairs):
+            first, second = 2 * p * LANES, (2 * p + 1) * LANES
+            upk[:, p * LANES : (p + 1) * LANES] = jnp.concatenate(
+                [vkv[:, first : first + NOPE], vkv[:, second : second + NOPE]], axis=1
+            )
+        turned = vkv[...].T
+        for h in range(heads):
+            upvt[h * VDIM : (h + 1) * VDIM] = turned[h * LANES + NOPE : (h + 1) * LANES]
 
     def raise_keys(src, slot, span):
         here = pl.ds(span[0] * chunk, len(span) * chunk)
@@ -293,10 +328,10 @@
         across_x = jnp.where(j < -1, i, lax.rem(x + step, nx))
         return (z - level) * nx + across_x, column
 
-    def pump(q):
+    def pump(q, low=0):
         k, r = q // count + 1, q % count
 
-        @pl.when(k <= z)
+        @pl.when(jnp.logical_and(k <= z, q >= low))
         def _():
             src = sp - k * nx
             arrival(src, r).wait_recv()
@@ -325,8 +360,10 @@
 
     def prepare(i):
         with jax.named_scope("pump"):
-            pump(5 + 2 * i)
-            pump(6 + 2 * i)
+            low = jnp.where(z < nz - 1, 6, 5)
+            first = 5 + 2 * (i - jnp.minimum(x, 1))
+            pump(first, low)
+            pump(first + 1, low)
         with jax.named_scope("fetch"):
             fetch(i + 2)
 
@@ -339,18 +376,15 @@
         with jax.named_scope(f"tokwait{r}"):
             if r == 0:
                 pass_on(r)
-            own_arrival(r).wait_recv()
             for step in range(1, ny):
                 forward_arrival(r, step).wait_recv()
-        if r == 0:
-            with jax.named_scope("wload2"):
-                for load in loads[2:5]:
-                    load.wait()
         here = part(r)
-        wide = jnp.concatenate([buf[s, here] for s in range(n)], axis=1).astype(F32)
-        factor = lax.rsqrt(jnp.sum(wide * wide, axis=1, keepdims=True) / (n * width) + EPSILON)
-        scaled = (wide * pre[...]).astype(BF)
-        scale_of[here] = scaled
+        square = near_square[here, :1]
+        for step in range(1, ny):
+            wide = pick(y_other(step), here)
+            square = square + jnp.sum(wide * wide, axis=1, keepdims=True)
+            far[step - 1, here] = (wide * pre[:, lanes_of(y_other(step))]).astype(BF)
+        factor = lax.rsqrt(square / (n * width) + EPSILON)
         factors[here] = jnp.broadcast_to(factor, (chunk, LANES))
         flat = jnp.broadcast_to(factor, (chunk, LANES)).T[:1]
         cosine, sine = angle[: ROPE // 2, here], angle[ROPE // 2 :, here]
@@ -360,10 +394,15 @@
                 [first * cosine - second * sine, second * cosine + first * sine], axis=0
             )
 
-        kv = dot(scaled, vk[...]) * factor
+        kv, key, q = near_k[here], near_r[:, here], near_q[here]
+        for step in range(1, ny):
+            scaled, there = far[step - 1, here], lanes_of(y_other(step))
+            kv = kv + dot(scaled, vk[there])
+            key = key + dot_nt(vr[:, there], scaled)
+        kv = kv * factor
         kv = kv * lax.rsqrt(jnp.mean(kv * kv, axis=1, keepdims=True) + EPSILON) * kg[...]
         kvs[sp, r, :chunk] = kv.astype(BF)
-        key = dot_nt(vr[...], scaled) * flat
+        key = key * flat
         key = rotate(key[: ROPE // 2], key[ROPE // 2 :])
         kvs[sp, r, chunk:] = jnp.concatenate(
             [key[g * TURN : (g + 1) * TURN] for g in range(ROPE // TURN)], axis=1
@@ -377,10 +416,9 @@
             def _(step=step):
                 own_side(r, step).start()
 
-        if r == 0:
-            with jax.named_scope("wload5"):
-                loads[5].wait()
-        q = dot(scaled, vq[...]) * factor
+        for step in range(1, ny):
+            q = q + dot(far[step - 1, here], vq[lanes_of(y_other(step))])
+        q = q * factor
         gains = jnp.concatenate([qg[i : i + 1] for i in range(qg.shape[0])], axis=1)
         q = q * lax.rsqrt(jnp.mean(q * q, axis=1, keepdims=True) + EPSILON) * gains
         with jax.named_scope("passon"):
@@ -403,9 +441,16 @@
 
     def branch(r):
         here = part(r)
-        scaled, factor = scale_of[here], factors[here, :1]
-        inner = (dot(scaled, vi[...]) * factor).astype(BF).astype(F32)
-        source = (dot(scaled, vs[...]) * factor).astype(BF).astype(F32)
+        factor = factors[here, :1]
+
+        def gate(index, w):
+            value = near_c[here, index * channels : (index + 1) * channels]
+            for step in range(1, ny):
+                value = value + dot(far[step - 1, here], w[lanes_of(y_other(step))])
+            return (value * factor).astype(BF)
+
+        inner = gate(0, vi).astype(F32)
+        source = gate(1, vs).astype(F32)
         driven = (inner * source).astype(BF)
         ext[8 + r * chunk : 8 + (r + 1) * chunk] = driven.astype(F32)
         if r == count - 1:
@@ -414,28 +459,31 @@
             @pl.when(sp < nsp - 1)
             def _():
                 halo_copy().start()
-        outer[here] = (dot(scaled, vo[...]) * factor).astype(BF)
+        outer[here] = gate(2, vo)
 
     for r in range(count):
         project(r)
-    with jax.named_scope("wload6"):
-        for load in loads[6:9]:
-            load.wait()
     with jax.named_scope("pump1"):
         pump(1)
     for r in range(count - 1, -1, -1):
         with jax.named_scope("branch"):
             branch(r)
+    with jax.named_scope("diag"):
+        do(raise_keys(sp, 0, list(range(count))))
+        units([(r, p, 0) for r in range(count - 1) for p in range(pairs)], True)
     with jax.named_scope("prefetch"):
         fetch(0)
         fetch(1)
         pump(2)
         pump(3)
     with jax.named_scope("diag"):
-        do(raise_keys(sp, 0, list(range(count))))
-        units([(r, p, 0) for r in range(count) for p in range(pairs)], True)
+        units([(count - 1, p, 0) for p in range(pairs)], True)
     with jax.named_scope("pump4"):
         pump(4)
+
+        @pl.when(z < nz - 1)
+        def _():
+            pump(5)
 
     everything = list(range(count))
     many = items >= WAVE
@@ -458,7 +506,17 @@
                     old[0] = old[1]
             return carry
 
-        lax.fori_loop(0, items - WAVE, whole, 0)
+        peel = jnp.logical_and(x == 0, items > WAVE)
+
+        @pl.when(peel)
+        def _():
+            with jax.named_scope("units"):
+                units([(c, p, 0) for c in everything for p in range(pairs)], False)
+            prepare(0)
+            shared(1)
+            do(raise_keys(place_of(1)[0], 0, everything))
+
+        lax.fori_loop(jnp.where(peel, 1, 0), items - WAVE, whole, 0)
         for w in range(WAVE - 1):
             prepare(items - WAVE + w)
             shared(items - WAVE + w + 1)
@@ -515,7 +573,7 @@
             sq.at[r], sqin.at[step, r], q_s.at[step - 1], q_r.at[r, step - 1], tp=lax.rem(tp + step, n)
         )
 
-    for load in loads[9:]:
+    for load in loads[12:]:
         load.wait()
 
     def send_on(c):
@@ -661,13 +719,17 @@
         outer_gate_weight, inner_gate_weight, source_weight, q_down_weight, kv_down_weight,
         rope_turned, q_up_weight, kv_up_weight, attn_out_weight, conv_out_weight,
     )
+    small = (
+        pre_gain[None], q_norm_gain.reshape(-1, LANES), kv_norm_gain[None], post_gain[None], conv_taps,
+    )
     block = (ny, rows, width)
     return pl.pallas_call(
         functools.partial(layer_kernel, nz, nx, ntp, chunk, heads),
         out_shape=[v((rows, width), BF), v((heads, rows), F32)],
-        in_specs=[anywhere] + [whole] * 5 + [anywhere] * (1 + len(weights)),
+        in_specs=[anywhere] * (7 + len(weights)),
         out_specs=[whole] * 2,
-        scratch_shapes=[v((ntp, rows, width), BF)]
+        scratch_shapes=[v(w.shape, w.dtype) for w in small]
+        + [v((ntp, rows, width), BF)]
         + [v(w.shape, BF) for w in weights]
         + [
             v((ROPE, rows), F32),
@@ -680,7 +742,9 @@
             v((AHEAD + 2, rows, 2 * chunk), F32),
             v((count, pairs, VDIM, 2 * chunk), F32),
             v((count, pairs, 1, 2 * chunk), F32), v((count, pairs, 1, 2 * chunk), F32),
-            v((rows, ntp * width), BF), v((rows, LANES), F32),
+            v((rows, 2 * width), BF), v((rows, LANES), F32), v((rows, rank), F32),
+            v((ROPE, rows), F32), v((rows, q_rank), F32), v((rows, 3 * channels), F32),
+            v((ny - 1, rows, 2 * width), BF), v((rows, LANES), F32),
             v((rows, channels), BF), v((8 + rows, channels), F32),
             v((HALO, channels), BF), v((HALO, channels), BF),
             v((rows, heads * VDIM + channels), BF),
@@ -689,7 +753,7 @@
         + [
             v((rows, width), BF), v((rows, width), BF), v((rows, width), F32),
             v((count, 8, chunk), F32), v((ntp, count, 8, chunk), F32),
-            DMA((count,)), DMA((11,)), DMA((1,)), DMA((count,)),
+            DMA((count,)), DMA((16,)), DMA((1,)), DMA((count,)),
             DMA((ny - 1,)), DMA((count, ny - 1)), DMA((ny - 1,)), DMA((count, ny - 1)),
             DMA((nz,)), DMA((nx - 1,)), DMA((nz - 1, nx - 1)),
             DMA((nsp, count)), DMA((nsp,)), DMA((nsp,)), DMA((1,)), DMA((1,)),
@@ -701,8 +765,7 @@
         ),
         name="layer",
     )(
-        tokens, pre_gain[None], q_norm_gain.reshape(-1, LANES), kv_norm_gain[None],
-        post_gain[None], conv_taps, jnp.asarray(angles(nsp * rows)), *weights,
+        tokens, *small, jnp.asarray(angles(nsp * rows)), *weights,
     )
 
 

time: 56.2 us -> 53.1 us (0.945)
  Pallas kernels: 53.9 us -> 50.5 us
    pallas_call x1, Pallas kernels: 53.9 us -> 50.5 us  [body(): pl.pallas_call(functools.partial(layer_kernel, nz, nx, ntp, chunk, heads)...]
where the time goes in v5:
time: 53.1 us; the launch traced here: 52.5 us
  Pallas kernels  50.5 us (95%)
  local copies, waits for them, and re-layouts  1.35 us (3%)
  between operations  0.65 us (1%)
    pallas_call x1, Pallas kernels, body(): pl.pallas_call(functools.partial(layer_kernel, nz, nx, ntp, chunk, heads)...  50.5 us
    unnamed x2, local copies, waits for them, and re-layouts  1.35 us

profile of v5, /device:TPU:27, one launch (start us, length us, event | category | flops | bytes accessed | tf_op | source)
XLA Modules:
  0.0 52.5 jit_solution(2423753132721217680)
XLA Ops:
  0.6 50.5 %layer.1 = (bf16[384,512]{1,0:T(8,128)(2,1)S(1)}, f32[8,384]{1,0:T(8,128)S(1)}) custom-call(bf16[384,512]{1,0:T(8,128)(2,1)} %tok.1, f32[1,2048]{1,0:T(1,128)} %bitcast.6, f32[6,128]{1,0:T(8,128)} %bitcast.7, f32[1,512]{1,0:T(1,128)} %bitcast.8, f32[1,512]{1,0:T(1,128)} %bitcast.9, bf16[3,256]{1,0:T(4,128)(2,1)} %taps_in.1, f32[32,3072]{1,0:T(8,128)} %constant.2.clone.table, ...), custom_call_target="tpu_custom_call" | custom-call | tf_op jit(solution)/shard_map/layer/pallas_call | solution.py:726
  51.2 0.7 %copy.21 = bf16[384,512]{1,0:T(8,128)(2,1)} copy(bf16[384,512]{1,0:T(8,128)(2,1)S(1)} %get-tuple-element.2) | data formatting | bytes 786432
  51.9 0.6 %copy.22 = f32[8,384]{1,0:T(8,128)} copy(f32[8,384]{1,0:T(8,128)S(1)} %get-tuple-element.3) | data formatting | bytes 24576
